TPU v7x, 128 devices: a whole 4x4x4 slice. The times are simulated.
128 devices in a mesh: sp: 16 (over z, x), tp: 8 (over y, core).
Axes of the slice: x: 4, y: 4, z: 4, core: 2. Of those that a mesh axis runs over, the one named last changes fastest.
Arguments:
- residual: bfloat16 [8192, 2048], P(('sp', 'tp')), may hold values from -6 to 6
- receptance_first: bfloat16 [8192, 1024], P('sp', 'tp'), may hold values from -6 to 6
- key_first_group: bfloat16 [8192, 1024], P('sp', 'tp'), may hold values from -6 to 6
- value_first_group: bfloat16 [8192, 1024], P('sp', 'tp'), may hold values from -6 to 6
- decay_preact_first: bfloat16 [8192, 1024], P('sp', 'tp'), may hold values from -5.5 to 5.5
- context_rate_first: bfloat16 [8192, 1024], P('sp', 'tp'), may hold values from -6 to 6
- decay_base_first: float32 [1024], P('tp'), may hold values from 9.9e-07 to 0.0301
- head_scale_first: float32 [1024], P('tp'), may hold values from 0.1 to 1.9
- receptance_second: bfloat16 [8192, 1024], P('sp', 'tp'), may hold values from -6 to 6
- key_second_group: bfloat16 [8192, 1024], P('sp', 'tp'), may hold values from -6 to 6
- value_second_group: bfloat16 [8192, 1024], P('sp', 'tp'), may hold values from -6 to 6
- decay_preact_second: bfloat16 [8192, 1024], P('sp', 'tp'), may hold values from -5.5 to 5.5
- context_rate_second: bfloat16 [8192, 1024], P('sp', 'tp'), may hold values from -6 to 6
- decay_base_second: float32 [1024], P('tp'), may hold values from 9.9e-07 to 0.0301
- head_scale_second: float32 [1024], P('tp'), may hold values from 0.1 to 1.9
- decay_extra_log: float32 [8192], P('sp'), may hold values from -0.7 to 0
- output_weight_first: bfloat16 [1024, 2048], P('tp'), may hold values from -0.125 to 0.125
- output_weight_second: bfloat16 [1024, 2048], P('tp'), may hold values from -0.125 to 0.125
- feedforward_gain: float32 [2048], replicated, may hold values from 0.1 to 1.9
- routed_expert_index: int32 [8192, 4], P(('sp', 'tp')), may hold values from 0 to 127, all different within a row; in each aligned block of 64 rows (0 to 63, 64 to 127, ...) at most 4 rows name the same one
- routed_expert_weight: float32 [8192, 4], P(('sp', 'tp')), may hold values from 0.2 to 1
- expert_gate_weight: bfloat16 [128, 2048, 512], P(('sp', 'tp')), may hold values from -0.125 to 0.125
- expert_up_weight: bfloat16 [128, 2048, 512], P(('sp', 'tp')), may hold values from -0.125 to 0.125
- expert_down_weight: bfloat16 [128, 512, 2048], P(('sp', 'tp')), may hold values from -0.25 to 0.25
- shared_gate_weight: bfloat16 [2048, 512], replicated, may hold values from -0.125 to 0.125
- shared_up_weight: bfloat16 [2048, 512], replicated, may hold values from -0.125 to 0.125
- shared_down_weight: bfloat16 [512, 2048], replicated, may hold values from -0.25 to 0.25
Outputs:
- layer_out: bfloat16 [8192, 2048], P(('sp', 'tp'))
Inputs may be any that keep to these rules, and one draw needn't show every extreme that they name: `routed_expert_index`: each row names 4 different experts. In each aligned block of the rows of one device, no expert is named by more than 4 rows, a bound that some block reaches.
All inputs are finite; a program needn't handle non-finite values.
Results may differ from a plain program's by a relative error of at most 0.013.
Values may be sent and summed in bfloat16 or wider, within the bound.
A program may use at most 128 MiB of HBM per device.

v0:
```python
import functools
import jax
import jax.numpy as jnp
from jax import lax
from jax.experimental import pallas as pl
from jax.experimental.pallas import tpu as pltpu
from jax.sharding import Mesh
from jax.sharding import PartitionSpec as P

F32, BF16 = jnp.float32, jnp.bfloat16
SPAN = 128
LANES = 128
KEY_EPSILON = 1e-06
HEAD_EPSILON = 0.00064
NORM_EPSILON = 1e-06


def nn(a, b):
    return lax.dot_general(a, b, (((1,), (0,)), ((), ())), preferred_element_type=F32)


def nt(a, b):
    return lax.dot_general(a, b, (((1,), (1,)), ((), ())), preferred_element_type=F32)


def halves(x):
    high = x.astype(BF16)
    return high, (x - high.astype(F32)).astype(BF16)


def dot1(f, a, b):
    return f(a.astype(BF16), b.astype(BF16))


def dot3(f, a, b):
    ah, al = halves(a)
    bh, bl = halves(b)
    return f(ah, bh) + (f(ah, bl) + f(al, bh))


def iota(shape, dim):
    return lax.broadcasted_iota(jnp.int32, shape, dim)


def head_sum(x, width):
    if width == LANES:
        return jnp.sum(x, axis=-1, keepdims=True)
    lane = iota(x.shape, 1)
    left = jnp.sum(jnp.where(lane < width, x, 0.0), axis=-1, keepdims=True)
    right = jnp.sum(jnp.where(lane < width, 0.0, x), axis=-1, keepdims=True)
    return jnp.where(lane < width, left, right)


def local_kernel(dot, *refs):
    (r_a, k_a, v_a, p_a, c_a, base_a, r_b, k_b, v_b, p_b, c_b, base_b, extra_ref) = refs[:13]
    read_a, map_a, read_b, map_b, message = refs[13:]
    square = (SPAN, SPAN)
    row, col = iota(square, 0), iota(square, 1)
    lower = row >= col
    strict = row > col
    lower_bf = jnp.where(lower, 1.0, 0.0).astype(BF16)
    eye = jnp.where(row == col, 1.0, 0.0)
    count = r_a.shape[0] // SPAN
    items = []
    for group, (r_, k_, v_, p_, c_, base_, width) in enumerate(
        ((r_a, k_a, v_a, p_a, c_a, base_a, 64), (r_b, k_b, v_b, p_b, c_b, base_b, 128))
    ):
        for block in range(count):
            at = pl.ds(block * SPAN, SPAN)
            key = k_[at, :].astype(F32)
            unit = key * lax.rsqrt(head_sum(key * key, width) + KEY_EPSILON)
            removal = unit * jax.nn.sigmoid(c_[at, :].astype(F32))
            slow = jax.nn.sigmoid(p_[at, :].astype(F32))
            extra = extra_ref[pl.ds(block, 1), :]
            rate = 2.0 * base_[...]
            high, low = halves(slow)
            run_slow = nn(lower_bf, high) + nn(lower_bf, low)
            run_extra = jnp.sum(jnp.where(lower, extra, 0.0), axis=-1, keepdims=True)
            own_extra = jnp.sum(jnp.where(row == col, extra, 0.0), axis=-1, keepdims=True)
            running = run_extra - rate * run_slow
            own_log = own_extra - rate * slow
            centre = running[SPAN // 2 - 1 : SPAN // 2, :]
            ending = running[SPAN - 1 : SPAN, :]
            grown = running - centre
            read = r_[at, :].astype(F32) * jnp.exp(grown)
            query = unit * jnp.exp(grown - own_log)
            write = removal * jnp.exp(-grown)
            write_end = write * jnp.exp(ending - centre)
            items.append(
                dict(
                    group=group,
                    block=block,
                    width=width,
                    read=read,
                    query=query,
                    write=write,
                    write_end=write_end,
                    value=v_[at, :].astype(F32),
                    centre=jnp.exp(centre),
                    ending=jnp.exp(ending),
                )
            )
    solves = []
    for item in items:
        lane = col < item["width"]
        masks = [None] if item["width"] == SPAN else [lane, jnp.logical_not(lane)]
        item["parts"] = []
        for mask in masks:
            query = item["query"] if mask is None else jnp.where(mask, item["query"], 0.0)
            read = item["read"] if mask is None else jnp.where(mask, item["read"], 0.0)
            both = dot(nt, jnp.concatenate([query, read], axis=0), item["write"])
            coupling = jnp.where(strict, both[:SPAN], 0.0)
            reading = jnp.where(lower, both[SPAN:], 0.0)
            part = dict(mask=mask, coupling=coupling, reading=reading)
            item["parts"].append(part)
            solves.append(part)
    size = 1
    while size < SPAN:
        near = ((row // (2 * size)) == (col // (2 * size))) & ((row // size) > (col // size))
        for part in solves:
            step = jnp.where(near, part["coupling"], 0.0)
            if size == 1:
                part["inverse"] = eye - step
            else:
                inverse = part["inverse"]
                part["inverse"] = inverse - dot(nn, dot(nn, inverse, step), inverse)
        size *= 2
    head_row, head_col = row < 64, col < 64
    same_head = head_row == head_col
    for item in items:
        parts = item["parts"]
        right = jnp.concatenate([item["value"], -item["query"]], axis=1)
        wide = iota(right.shape, 1) % SPAN < 64

        def spread(x):
            if len(parts) == 1:
                return x
            return jnp.concatenate([jnp.where(wide, x, 0.0), jnp.where(wide, 0.0, x)], axis=0)

        def joined(name):
            return jnp.concatenate([part[name] for part in parts], axis=1)

        solved = dot(nn, joined("inverse"), spread(right))
        given = dot(nn, joined("reading"), spread(solved))
        item["local_read"] = given[:, :SPAN]
        item["state_read"] = (item["read"] + given[:, SPAN:]) * item["centre"]
        scaled = jnp.concatenate([solved[:, :SPAN], solved[:, SPAN:] * item["centre"]], axis=1)
        step = dot(nn, item["write_end"].T, scaled)
        diagonal = jnp.where(row == col, item["ending"], 0.0)
        step = step + jnp.concatenate([jnp.zeros(square, F32), diagonal], axis=1)
        if item["width"] < SPAN:
            both_heads = jnp.concatenate([same_head, same_head], axis=1)
            step = jnp.where(both_heads, step, 0.0)
        item["step"] = step
    for group, (read_ref, map_ref) in enumerate(((read_a, map_a), (read_b, map_b))):
        held = None
        for item in items:
            if item["group"] != group:
                continue
            at = pl.ds(item["block"] * SPAN, SPAN)
            if held is None:
                read_ref[at, :] = item["local_read"]
                map_ref[at, :] = item["state_read"].astype(BF16)
                held = item["step"]
            else:
                out = dot(nn, item["state_read"], held)
                read_ref[at, :] = item["local_read"] + out[:, :SPAN]
                map_ref[at, :] = out[:, SPAN:].astype(BF16)
                step = item["step"]
                held = dot(nn, step[:, SPAN:], held)
                held = jnp.concatenate([held[:, :SPAN] + step[:, :SPAN], held[:, SPAN:]], axis=1)
        if group == 0:
            message[0:64, :] = (held[:64, :] + held[64:, :]).astype(BF16)
        else:
            message[64:192, :] = held.astype(BF16)


def local_call(args, dot=dot1):
    rows = args[0].shape[0]
    shapes = [
        jax.ShapeDtypeStruct((rows, LANES), F32),
        jax.ShapeDtypeStruct((rows, LANES), BF16),
        jax.ShapeDtypeStruct((rows, LANES), F32),
        jax.ShapeDtypeStruct((rows, LANES), BF16),
        jax.ShapeDtypeStruct((192, 2 * LANES), BF16),
    ]
    return pl.pallas_call(
        functools.partial(local_kernel, dot),
        out_shape=shapes,
        in_specs=[pl.BlockSpec(memory_space=pltpu.VMEM)] * 13,
        out_specs=[pl.BlockSpec(memory_space=pltpu.VMEM)] * 5,
        name="local_terms",
    )(*args)


Z, X, Y, C = "z", "x", "y", "core"
ALL = (Z, X, Y, C)
MESH = pl.DeviceIdType.MESH
VMEM = pltpu.VMEM


def whole(count):
    return [pl.BlockSpec(memory_space=pltpu.VMEM)] * count


def greet(peers):
    barrier = pltpu.get_barrier_semaphore()
    for peer in peers:
        pl.semaphore_signal(barrier, inc=1, device_id=peer, device_id_type=MESH)
    pl.semaphore_wait(barrier, len(peers))


def follow(step, held):
    high, low = halves(held)
    moved = nn(step[:, LANES:], high) + nn(step[:, LANES:], low)
    return moved


def exchange_kernel(
    message, enter_a, enter_b, rows, columns, total, row_send, row_recv, col_send, col_recv
):
    z, x, y, c = [lax.axis_index(name) for name in ALL]
    row_peers = [(z, lax.rem(x + d, 4), y, c) for d in range(1, 4)]
    col_peers = [(lax.rem(z + d, 4), x, y, c) for d in range(1, 4)]
    greet(row_peers + col_peers)

    def row_copy(d):
        return pltpu.make_async_remote_copy(
            src_ref=message,
            dst_ref=rows.at[d],
            send_sem=row_send.at[d],
            recv_sem=row_recv.at[d],
            device_id=row_peers[d - 1],
            device_id_type=MESH,
        )

    def col_copy(d):
        return pltpu.make_async_remote_copy(
            src_ref=total,
            dst_ref=columns.at[d],
            send_sem=col_send.at[d],
            recv_sem=col_recv.at[d],
            device_id=col_peers[d - 1],
            device_id_type=MESH,
        )

    for d in (2, 1, 3):
        row_copy(d).start()
    rows[0] = message[...]
    square = (LANES, 2 * LANES)
    row, col = iota(square, 0), iota(square, 1)
    same = (row < 64) == (col % LANES < 64)
    unit = jnp.where(row + LANES == col, 1.0, 0.0)
    for d in range(1, 4):
        row_copy(d).wait()

    def steps(packed):
        top = packed[0:64, :]
        first = jnp.where(same, jnp.concatenate([top, top], axis=0), jnp.zeros((), BF16))
        return first, packed[64:192, :]

    def chain(step, held):
        moved = follow(step, held)
        own = step[:, :LANES].astype(F32)
        return jnp.concatenate([moved[:, :LANES] + own, moved[:, LANES:]], axis=1)

    inside = [unit, unit]
    running = [unit, unit]
    for k in range(4):
        pair = steps(rows[lax.rem(x - k + 4, 4)])
        inside = [jnp.where(x == k, now, old) for now, old in zip(running, inside)]
        if k == 0:
            running = [p.astype(F32) for p in pair]
        else:
            running = [chain(p, r) for p, r in zip(pair, running)]
    total[0:64, :] = (running[0][:64, :] + running[0][64:, :]).astype(BF16)
    total[64:192, :] = running[1].astype(BF16)
    for d in (2, 1, 3):

        @pl.when(z + d < 4)
        def _():
            col_copy(d).start()

    enter_a[...] = jnp.zeros_like(enter_a)
    enter_b[...] = jnp.zeros_like(enter_b)
    for k in range(3):

        @pl.when(k < z)
        def _():
            d = z - k
            pltpu.make_async_remote_copy(
                src_ref=total,
                dst_ref=columns.at[d],
                send_sem=col_send.at[d],
                recv_sem=col_recv.at[d],
                device_id=(k, x, y, c),
                device_id_type=MESH,
            ).wait_recv()
            pair = steps(columns[d])
            for enter, step in zip((enter_a, enter_b), pair):
                enter[...] = follow(step, enter[...]) + step[:, :LANES].astype(F32)

    for enter, own in zip((enter_a, enter_b), inside):
        enter[...] = dot3(nn, own[:, LANES:], enter[...]) + own[:, :LANES]
    for d in (2, 1, 3):

        @pl.when(z + d < 4)
        def _():
            col_copy(d).wait_send()


def exchange_call(message):
    shape = jax.ShapeDtypeStruct((LANES, LANES), F32)
    return pl.pallas_call(
        exchange_kernel,
        out_shape=[shape, shape],
        in_specs=whole(1),
        out_specs=whole(2),
        scratch_shapes=[
            pltpu.VMEM((4, 192, 2 * LANES), BF16),
            pltpu.VMEM((4, 192, 2 * LANES), BF16),
            pltpu.VMEM((192, 2 * LANES), BF16),
        ]
        + [pltpu.SemaphoreType.DMA((4,))] * 4,
        compiler_params=pltpu.CompilerParams(collective_id=1, has_side_effects=True),
        name="exchange",
    )(message)


def project_kernel(
    read_a, map_a, enter_a, gain_a, weight_a, read_b, map_b, enter_b, gain_b, weight_b, out
):
    square = (LANES, LANES)
    row, col = iota(square, 0), iota(square, 1)
    mixed = []
    for read, map_, enter, gain, width in (
        (read_a, map_a, enter_a, gain_a, 64),
        (read_b, map_b, enter_b, gain_b, 128),
    ):
        mean = jnp.where((row // width) == (col // width), 1.0 / width, 0.0).astype(BF16)
        high, low = halves(enter[...])
        readout = read[...] + nn(map_[...], high) + nn(map_[...], low)
        high, low = halves(readout)
        centred = readout - (nn(high, mean) + nn(low, mean))
        high, low = halves(centred * centred)
        spread = nn(high, mean) + nn(low, mean)
        mixed.append((centred * lax.rsqrt(spread + HEAD_EPSILON) * gain[...]).astype(BF16))
    rows, width = out.shape
    both = jnp.concatenate(mixed, axis=1)
    weight = jnp.concatenate([weight_a[...], weight_b[...]], axis=0)
    for at in range(0, width, 512):
        out[:, at : at + 512] = nn(both, weight[:, at : at + 512]).astype(BF16)


def project_call(args, rows, width):
    return pl.pallas_call(
        project_kernel,
        out_shape=jax.ShapeDtypeStruct((rows, width), BF16),
        in_specs=whole(10),
        out_specs=whole(1)[0],
        name="project",
    )(*args)


def scatter_kernel(part, out, pair_in, own, ring_in, pair_send, pair_recv, ring_send, ring_recv):
    z, x, y, c = [lax.axis_index(name) for name in ALL]
    partner = (z, x, y, 1 - c)
    peers = [(z, x, lax.rem(y + d, 4), c) for d in range(1, 4)]
    greet([partner] + peers)
    rows = out.shape[0]

    def pair_copy(d):
        goal = lax.rem(y + d, 4)
        return pltpu.make_async_remote_copy(
            src_ref=part.at[goal * 2 + (1 - c)],
            dst_ref=pair_in.at[d],
            send_sem=pair_send.at[d],
            recv_sem=pair_recv.at[d],
            device_id=partner,
            device_id_type=MESH,
        )

    def ring_copy(d):
        return pltpu.make_async_remote_copy(
            src_ref=own.at[d],
            dst_ref=ring_in.at[d],
            send_sem=ring_send.at[d],
            recv_sem=ring_recv.at[d],
            device_id=peers[d - 1],
            device_id_type=MESH,
        )

    for d in (2, 1, 3, 0):
        pair_copy(d).start()
    for d in (2, 1, 3):
        pair_copy(d).wait()
        goal = lax.rem(y + d, 4)
        own[d] = (part[goal * 2 + c].astype(F32) + pair_in[d].astype(F32)).astype(BF16)
        ring_copy(d).start()
    pair_copy(0).wait()
    out[...] = part[y * 2 + c].astype(F32) + pair_in[0].astype(F32)
    for d in (1, 3, 2):
        ring_copy(d).wait()
        out[...] += ring_in[d].astype(F32)


def scatter_call(part):
    blocks, rows, width = part.shape
    return pl.pallas_call(
        scatter_kernel,
        out_shape=jax.ShapeDtypeStruct((rows, width), F32),
        in_specs=whole(1),
        out_specs=whole(1)[0],
        scratch_shapes=[pltpu.VMEM((4, rows, width), BF16)] * 3
        + [pltpu.SemaphoreType.DMA((4,))] * 4,
        compiler_params=pltpu.CompilerParams(collective_id=2, has_side_effects=True),
        name="scatter_sum",
    )(part)


SLOTS = 4
PARTS = 4
UNIT = SLOTS * PARTS


def routing(index):
    rows, top = index.shape
    experts = iota((rows, LANES), 1)
    chosen = jnp.zeros((rows, LANES), F32)
    for k in range(top):
        chosen += jnp.where(index[:, k : k + 1] == experts, 1.0, 0.0)
    earlier = jnp.where(iota((rows, rows), 0) > iota((rows, rows), 1), 1.0, 0.0).astype(BF16)
    rank = nn(earlier, chosen.astype(BF16))
    code = (chosen * (rank + 1.0)).astype(BF16)
    return jnp.concatenate([code] * PARTS, axis=0)


def dispatch_kernel(residual, summed, gain, index, attended, normed, sent):
    total = (residual[...].astype(F32) + summed[...]).astype(BF16)
    attended[...] = total
    wide = total.astype(F32)
    mean = jnp.mean(wide * wide, axis=-1, keepdims=True)
    rows_ = (wide * lax.rsqrt(mean + NORM_EPSILON) * gain[...]).astype(BF16)
    normed[...] = rows_
    rows, width = rows_.shape
    part = width // PARTS
    stacked = jnp.concatenate([rows_[:, q * part : (q + 1) * part] for q in range(PARTS)], axis=0)
    code = routing(index)
    shape = (256, PARTS * rows)
    place = iota(shape, 0) % UNIT
    fits = (place // SLOTS) == (iota(shape, 1) // rows)
    wanted = (place % SLOTS + 1).astype(F32)
    for k in range(sent.shape[0] // 256):
        select = (iota((256, LANES), 0) + 256 * k) // UNIT == iota((256, LANES), 1)
        found = nt(jnp.where(select, 1.0, 0.0).astype(BF16), code)
        taken = jnp.where(fits & (found == wanted), 1.0, 0.0).astype(BF16)
        sent[256 * k : 256 * (k + 1), :] = nn(taken, stacked).astype(BF16)


def dispatch_call(residual, summed, gain, index, devices):
    rows, width = residual.shape
    return pl.pallas_call(
        dispatch_kernel,
        out_shape=[
            jax.ShapeDtypeStruct((rows, width), BF16),
            jax.ShapeDtypeStruct((rows, width), BF16),
            jax.ShapeDtypeStruct((devices * UNIT, width // PARTS), BF16),
        ],
        in_specs=whole(4),
        out_specs=whole(3),
        name="dispatch",
    )(residual, summed, gain, index)


def expert_kernel(arrived, gate, up, down, out, rows_, hidden):
    part = arrived.shape[1]
    groups = arrived.shape[0] // 256
    a, b = iota((256, 256), 0), iota((256, 256), 1)
    here = (b % UNIT // SLOTS) * 64 + (b // UNIT) * SLOTS + b % SLOTS
    order = jnp.where(a == here, 1.0, 0.0).astype(BF16)
    there = (a % UNIT // SLOTS) * 64 + (a // UNIT) * SLOTS + a % SLOTS
    back = jnp.where(b == there, 1.0, 0.0).astype(BF16)
    for k in range(groups):
        sorted_ = nn(order, arrived[256 * k : 256 * (k + 1), :]).astype(BF16)
        for q in range(PARTS):
            rows_[64 * k : 64 * (k + 1), q * part : (q + 1) * part] = sorted_[64 * q : 64 * (q + 1)]
    for at in range(0, hidden.shape[1], 256):
        gate_val = nn(rows_[...], gate[:, at : at + 256])
        up_val = nn(rows_[...], up[:, at : at + 256])
        hidden[:, at : at + 256] = (gate_val * jax.nn.sigmoid(gate_val) * up_val).astype(BF16)
    for at in range(0, rows_.shape[1], 512):
        rows_[:, at : at + 512] = nn(hidden[...], down[:, at : at + 512]).astype(BF16)
    for k in range(groups):
        stacked = jnp.concatenate(
            [rows_[64 * k : 64 * (k + 1), q * part : (q + 1) * part] for q in range(PARTS)], axis=0
        )
        out[256 * k : 256 * (k + 1), :] = nn(back, stacked).astype(BF16)


def expert_call(arrived, gate, up, down):
    slots = arrived.shape[0] // PARTS
    return pl.pallas_call(
        expert_kernel,
        out_shape=jax.ShapeDtypeStruct(arrived.shape, BF16),
        in_specs=whole(4),
        out_specs=whole(1)[0],
        scratch_shapes=[
            pltpu.VMEM((slots, gate.shape[0]), BF16),
            pltpu.VMEM((slots, gate.shape[1]), BF16),
        ],
        compiler_params=pltpu.CompilerParams(vmem_limit_bytes=60 * 1024 * 1024),
        name="expert",
    )(arrived, gate, up, down)


def combine_kernel(attended, shared, returned, index, weights, out):
    rows, width = attended.shape
    part = width // PARTS
    code = routing(index)
    experts = iota((rows, LANES), 1)
    scale = jnp.zeros((rows, LANES), F32)
    for k in range(index.shape[1]):
        scale += jnp.where(index[:, k : k + 1] == experts, weights[:, k : k + 1], 0.0)
    high, low = halves(jnp.concatenate([scale] * PARTS, axis=0))
    shape = (PARTS * rows, 256)
    place = iota(shape, 1) % UNIT
    fits = (place // SLOTS) == (iota(shape, 0) // rows)
    wanted = (place % SLOTS + 1).astype(F32)
    routed = jnp.zeros((PARTS * rows, part), F32)
    for k in range(returned.shape[0] // 256):
        select = (iota((256, LANES), 0) + 256 * k) // UNIT == iota((256, LANES), 1)
        select = jnp.where(select, 1.0, 0.0).astype(BF16)
        match = fits & (nt(code, select) == wanted)
        block = returned[256 * k : 256 * (k + 1), :]
        routed += nn(jnp.where(match, nt(high, select), 0.0).astype(BF16), block)
        routed += nn(jnp.where(match, nt(low, select), 0.0).astype(BF16), block)
    for q in range(PARTS):
        at = slice(q * part, (q + 1) * part)
        out[:, at] = (
            attended[:, at].astype(F32) + shared[:, at] + routed[q * rows : (q + 1) * rows, :]
        ).astype(BF16)


def combine_call(attended, shared, returned, index, weights):
    return pl.pallas_call(
        combine_kernel,
        out_shape=jax.ShapeDtypeStruct(attended.shape, BF16),
        in_specs=whole(5),
        out_specs=whole(1)[0],
        name="combine",
    )(attended, shared, returned, index, weights)


def swap_kernel(source, out, send, recv, own_sem):
    z, x, y, c = [lax.axis_index(name) for name in ALL]
    me = ((z * 4 + x) * 4 + y) * 2 + c
    devices = source.shape[0] // UNIT

    def block(k):
        return pl.ds(pl.multiple_of(k * UNIT, UNIT), UNIT)

    def copy(d):
        dz, dx, dy, dc = d % 4, d // 4 % 4, d // 16 % 4, d // 64
        pz, px, py, pc = (z + dz) % 4, (x + dx) % 4, (y + dy) % 4, (c + dc) % 2
        peer = ((pz * 4 + px) * 4 + py) * 2 + pc
        sz, sx, sy, sc = (z - dz + 4) % 4, (x - dx + 4) % 4, (y - dy + 4) % 4, (c - dc + 2) % 2
        giver = ((sz * 4 + sx) * 4 + sy) * 2 + sc
        start = pltpu.make_async_remote_copy(
            src_ref=source.at[block(peer)],
            dst_ref=out.at[block(me)],
            send_sem=send.at[d],
            recv_sem=recv.at[d],
            device_id=(pz, px, py, pc),
            device_id_type=MESH,
        )
        arrive = pltpu.make_async_remote_copy(
            src_ref=source.at[block(peer)],
            dst_ref=out.at[block(giver)],
            send_sem=send.at[d],
            recv_sem=recv.at[d],
            device_id=(pz, px, py, pc),
            device_id_type=MESH,
        )
        return start, arrive

    @pl.loop(1, devices)
    def _(d):
        copy(d)[0].start()

    out[block(me), :] = source[block(me), :]

    @pl.loop(1, devices)
    def _(d):
        copy(d)[1].wait()


def swap_call(source):
    devices = source.shape[0] // UNIT
    return pl.pallas_call(
        swap_kernel,
        out_shape=jax.ShapeDtypeStruct(source.shape, BF16),
        in_specs=whole(1),
        out_specs=whole(1)[0],
        scratch_shapes=[pltpu.SemaphoreType.DMA((devices,))] * 2 + [pltpu.SemaphoreType.DMA],
        compiler_params=pltpu.CompilerParams(has_side_effects=True),
        name="swap",
    )(source)


def swiglu_hidden(inputs, w_gate, w_up):
    gate_val = jnp.dot(inputs, w_gate, preferred_element_type=F32)
    up_val = jnp.dot(inputs, w_up, preferred_element_type=F32)
    return (jax.nn.silu(gate_val) * up_val).astype(BF16)


def exchange_slots(slots):
    devices = slots.shape[0] // UNIT
    return lax.all_to_all(
        slots.reshape(devices, UNIT, -1), ALL, split_axis=0, concat_axis=0, tiled=True
    ).reshape(slots.shape)


def local(
    residual,
    receptance_first,
    key_first_group,
    value_first_group,
    decay_preact_first,
    context_rate_first,
    decay_base_first,
    head_scale_first,
    receptance_second,
    key_second_group,
    value_second_group,
    decay_preact_second,
    context_rate_second,
    decay_base_second,
    head_scale_second,
    decay_extra_log,
    output_weight_first,
    output_weight_second,
    feedforward_gain,
    routed_expert_index,
    routed_expert_weight,
    expert_gate_weight,
    expert_up_weight,
    expert_down_weight,
    shared_gate_weight,
    shared_up_weight,
    shared_down_weight,
):
    rows = receptance_first.shape[0]
    width = residual.shape[1]
    read_a, map_a, read_b, map_b, message = local_call(
        (
            receptance_first,
            key_first_group,
            value_first_group,
            decay_preact_first,
            context_rate_first,
            decay_base_first[None, :],
            receptance_second,
            key_second_group,
            value_second_group,
            decay_preact_second,
            context_rate_second,
            decay_base_second[None, :],
            decay_extra_log.reshape(-1, SPAN),
        )
    )
    enter_a, enter_b = exchange_call(message)
    partial = project_call(
        (
            read_a,
            map_a,
            enter_a,
            head_scale_first[None, :],
            output_weight_first,
            read_b,
            map_b,
            enter_b,
            head_scale_second[None, :],
            output_weight_second,
        ),
        rows,
        width,
    )
    summed = scatter_call(partial.reshape(-1, residual.shape[0], width))
    devices = lax.axis_size(ALL)
    attended, normed, slots = dispatch_call(
        residual, summed, feedforward_gain[None, :], routed_expert_index, devices
    )
    arrived = exchange_slots(slots)
    result = expert_call(
        arrived, expert_gate_weight[0], expert_up_weight[0], expert_down_weight[0]
    )
    returned = exchange_slots(result)
    shared_out = jnp.dot(
        swiglu_hidden(normed, shared_gate_weight, shared_up_weight),
        shared_down_weight,
        preferred_element_type=F32,
    )
    return combine_call(attended, shared_out, returned, routed_expert_index, routed_expert_weight)


def solution(mesh):
    finer = Mesh(mesh.devices.reshape(4, 4, 4, 2), ALL)
    sp, tp = (Z, X), (Y, C)
    heads = (P(sp, tp),) * 5 + (P(tp),) * 2
    placed = (
        (P(ALL, None),)
        + heads
        + heads
        + (P(sp), P(tp, None), P(tp, None), P(), P(ALL, None), P(ALL, None))
        + (P(ALL, None, None),) * 3
        + (P(),) * 3
    )
    return jax.shard_map(
        local, mesh=finer, in_specs=placed, out_specs=P(ALL, None), check_vma=False
    )
```

profile of v0, /device:TPU:1, one launch (start us, length us, event | category | flops | bytes accessed | tf_op | source)
XLA Modules:
  0.0 147.1 jit_solution(6506699595505516659)
XLA Ops:
  0.0 0.0 copy-start
  0.0 1.5 %copy.28.index = s32[64,4]{1,0:T(8,128)} copy(s32[64,4]{0,1:T(4,128)} %param.46) | data formatting | bytes 2048 | tf_op args[19]
  1.5 7.0 %local_terms.1 = (f32[512,128]{1,0:T(8,128)}, bf16[512,128]{1,0:T(8,128)(2,1)}, f32[512,128]{1,0:T(8,128)}, bf16[512,128]{1,0:T(8,128)(2,1)}, bf16[192,256]{1,0:T(8,128)(2,1)}) custom-call(bf16[512,128]{1,0:T(8,128)(2,1)} %refs_0_.1, bf16[512,128]{1,0:T(8,128)(2,1)} %refs_1_.1, bf16[512,128]{1,0:T(8,128)(2,1)} %refs_2_.1, bf16[512,128]{1,0:T(8,128)(2,1)} %refs_3_.1, ...), custom_call_target="tpu_custom_call" | custom-call | tf_op jit(solution)/shard_map/local_terms/pallas_call | solution.py:187
  8.5 18.7 %exchange.1 = (f32[128,128]{1,0:T(8,128)}, f32[128,128]{1,0:T(8,128)}) custom-call(bf16[192,256]{1,0:T(8,128)(2,1)} %get-tuple-element.17.message), custom_call_target="tpu_custom_call" | custom-call | tf_op jit(solution)/shard_map/exchange/pallas_call | solution.py:314
  27.2 4.5 %project.1 = bf16[512,2048]{1,0:T(8,128)(2,1)} custom-call(f32[512,128]{1,0:T(8,128)} %get-tuple-element.15.read_a, bf16[512,128]{1,0:T(8,128)(2,1)} %get-tuple-element.16.map_a, f32[128,128]{1,0:T(8,128)} %get-tuple-element.18.enter_a, f32[1,128]{1,0:T(1,128)} %bitcast.30, bf16[128,2048]{1,0:T(8,128)(2,1)} %weight_a.1, ...), custom_call_target="tpu_custom_call" | custom-call | tf_op jit(solution)/shard_map/project/pallas_call | solution.py:356
  31.7 21.4 %scatter_sum.1.summed = f32[64,2048]{1,0:T(8,128)} custom-call(bf16[8,64,2048]{2,1,0:T(8,128)(2,1)} %bitcast.21), custom_call_target="tpu_custom_call" | custom-call | tf_op jit(solution)/shard_map/scatter_sum/pallas_call | solution.py:409
  53.1 4.5 %dispatch.1 = (bf16[64,2048]{1,0:T(8,128)(2,1)}, bf16[64,2048]{1,0:T(8,128)(2,1)}, bf16[2048,512]{1,0:T(8,128)(2,1)}) custom-call(bf16[64,2048]{1,0:T(8,128)(2,1)} %residual.1, f32[64,2048]{1,0:T(8,128)} %scatter_sum.1.summed, f32[1,2048]{1,0:T(1,128)} %bitcast.26, s32[64,4]{1,0:T(8,128)} %copy.28.index), custom_call_target="tpu_custom_call" | custom-call | tf_op jit(solution)/shard_map/dispatch/pallas_call | solution.py:462
  57.7 37.8 %all_to_all.10 = bf16[128,16,512]{2,1,0:T(8,128)(2,1)} all-to-all(bf16[128,16,512]{2,1,0:T(8,128)(2,1)} %bitcast.25), channel_id=1, replica_groups=mesh['z'=4,'x'=4,'y'=4,'core'=2] {'z','x','y','core'}, dimensions={0} | all-to-all | bytes 4194304 | tf_op jit(solution)/shard_map/all_to_all | solution.py:618
  95.5 9.3 %expert.1 = bf16[2048,512]{1,0:T(8,128)(2,1)} custom-call(bf16[2048,512]{1,0:T(8,128)(2,1)} %bitcast.20, bf16[2048,512]{1,0:T(8,128)(2,1)} %bitcast.22, bf16[2048,512]{1,0:T(8,128)(2,1)} %bitcast.23, bf16[512,2048]{1,0:T(8,128)(2,1)} %bitcast.24), custom_call_target="tpu_custom_call" | custom-call | tf_op jit(solution)/shard_map/expert/pallas_call | solution.py:502
  104.8 0.0 copy-start.2
  104.8 0.0 copy-start.1
  104.8 6.1 %all-to-all-start.1 = ((bf16[128,16,512]{2,1,0:T(8,128)(2,1)}), bf16[128,16,512]{2,1,0:T(8,128)(2,1)}, u32[]{:S(2)}, u32[]{:S(2)}) async-start(bf16[128,16,512]{2,1,0:T(8,128)(2,1)} %bitcast.19), calls=%async_computation.1 | async-start | bytes 4194304 | tf_op jit(solution)/shard_map/all_to_all | solution.py:618
  110.9 0.0 copy-done.2
  110.9 0.7 copy.30.weights
  111.6 0.0 copy-done.1
  111.6 2.1 %fusion.9 = f32[64,512]{1,0:T(8,128)S(1)} fusion(bf16[64,2048]{1,0:T(8,128)(2,1)S(1)} %copy-done.1, bf16[2048,512]{1,0:T(8,128)(2,1)} %param.51), kind=kOutput, calls=%fused_computation.10 | convolution fusion | flops 134217728 | bytes 2490368 | tf_op jit(solution)/shard_map/dot_general | solution.py:611
  113.7 0.0 copy-done
  113.7 3.3 %fusion.1.shared = f32[64,2048]{1,0:T(8,128)} fusion(bf16[512,2048]{1,0:T(8,128)(2,1)S(1)} %copy-done, bf16[64,2048]{1,0:T(8,128)(2,1)S(1)} %copy-done.1, bf16[2048,512]{1,0:T(8,128)(2,1)} %param.52, f32[64,512]{1,0:T(8,128)S(1)} %fusion.9), kind=kOutput, calls=%fused_computation.2 | convolution fusion | flops 268632064 | bytes 5111808 | tf_op jit(solution)/shard_map/dot_general | solution.py:698
  117.0 23.8 %all-to-all-done.1 = bf16[128,16,512]{2,1,0:T(8,128)(2,1)} async-done(((bf16[128,16,512]{2,1,0:T(8,128)(2,1)}), bf16[128,16,512]{2,1,0:T(8,128)(2,1)}, u32[]{:S(2)}, u32[]{:S(2)}) %all-to-all-start.1) | async-done | bytes 2097184 | tf_op jit(solution)/shard_map/all_to_all | solution.py:618
  140.8 6.2 %combine.1 = bf16[64,2048]{1,0:T(8,128)(2,1)} custom-call(bf16[64,2048]{1,0:T(8,128)(2,1)} %get-tuple-element.22.attended, f32[64,2048]{1,0:T(8,128)} %fusion.1.shared, bf16[2048,512]{1,0:T(8,128)(2,1)} %bitcast.13.returned, s32[64,4]{1,0:T(8,128)} %copy.28.index, f32[64,4]{1,0:T(8,128)} %copy.30.weights), custom_call_target="tpu_custom_call" | custom-call | tf_op jit(solution)/shard_map/combine/pallas_call | solution.py:545
Async XLA Ops:
  0.0 113.7 %copy-start = (bf16[512,2048]{1,0:T(8,128)(2,1)S(1)}, bf16[512,2048]{1,0:T(8,128)(2,1)}, u32[]{:S(2)}) copy-start(bf16[512,2048]{1,0:T(8,128)(2,1)} %param.53) | copy-start | bytes 6291460
  104.8 6.1 %copy-start.2 = (f32[64,4]{0,1:T(4,128)S(1)}, f32[64,4]{0,1:T(4,128)}, u32[]{:S(2)}) copy-start(f32[64,4]{0,1:T(4,128)} %param.47) | copy-start | bytes 3076
  104.8 6.8 %copy-start.1 = (bf16[64,2048]{1,0:T(8,128)(2,1)S(1)}, bf16[64,2048]{1,0:T(8,128)(2,1)}, u32[]{:S(2)}) copy-start(bf16[64,2048]{1,0:T(8,128)(2,1)} %get-tuple-element.23) | copy-start | bytes 786436
  104.8 36.0 %all-to-all-start.1 = ((bf16[128,16,512]{2,1,0:T(8,128)(2,1)}), bf16[128,16,512]{2,1,0:T(8,128)(2,1)}, u32[]{:S(2)}, u32[]{:S(2)}) async-start(bf16[128,16,512]{2,1,0:T(8,128)(2,1)} %bitcast.19), calls=%async_computation.1 | async-start | bytes 4194304 | tf_op jit(solution)/shard_map/all_to_all | solution.py:618
where the time goes:
time: 148 us; the launch traced here: 147 us
  Pallas kernels  71.7 us (48%)
  blocking collectives  37.8 us (26%)
  waiting for transfers between devices  23.8 us (16%)
  starting transfers between devices  6.11 us (4%)
  matrix products  5.37 us (4%)
  local copies, waits for them, and re-layouts  2.22 us (2%)
    all_to_all x1, blocking collectives, exchange_slots(): lax.all_to_all(slots.reshape(devices, UNIT, -1), ALL, split_axis=0, conca...  37.8 us
    all_to_all x1, waiting for transfers between devices, exchange_slots(): lax.all_to_all(slots.reshape(devices, UNIT, -1), ALL, split_axis=0, conca...  23.8 us
    pallas_call x1, Pallas kernels, scatter_call(): pl.pallas_call(scatter_kernel, out_shape=jax.ShapeDtypeStruct((rows, widt...  21.4 us
    pallas_call x1, Pallas kernels, exchange_call(): pl.pallas_call(exchange_kernel, out_shape=[shape, shape], in_specs=whole(...  18.7 us
    pallas_call x1, Pallas kernels, expert_call(): pl.pallas_call(expert_kernel, out_shape=jax.ShapeDtypeStruct(arrived.shap...  9.31 us
    pallas_call x1, Pallas kernels, local_call(): pl.pallas_call(functools.partial(local_kernel, dot), out_shape=shapes, in...  6.99 us
    pallas_call x1, Pallas kernels, combine_call(): pl.pallas_call(combine_kernel, out_shape=jax.ShapeDtypeStruct(attended.sh...  6.25 us
    all_to_all x1, starting transfers between devices, exchange_slots(): lax.all_to_all(slots.reshape(devices, UNIT, -1), ALL, split_axis=0, conca...  6.11 us
  transfers between devices with their start and end apart: 1, of which 1 were waited for; matrix products, arithmetic and copies ran while one was open for 4% of the time, Pallas kernels for 0%

commit v1 on v0

--- a/solution.py
+++ b/solution.py
@@ -1,6 +1,9 @@
 import functools
+import itertools
+
 import jax
 import jax.numpy as jnp
+import numpy as np
 from jax import lax
 from jax.experimental import pallas as pl
 from jax.experimental.pallas import tpu as pltpu
@@ -423,201 +426,257 @@
 UNIT = SLOTS * PARTS
 
 
-def routing(index):
-    rows, top = index.shape
-    experts = iota((rows, LANES), 1)
+DISTANCE = lambda move: sum(min(step, 4 - step) for step in move[:3])
+MOVES = sorted(
+    itertools.product(range(4), range(4), range(4), range(2)),
+    key=lambda move: (-DISTANCE(move), -move[3]),
+)
+GROUP = 256
+CHUNKS = 4
+
+
+def shift(position, move, sign):
+    moved = []
+    for at, step, size in zip(position, move, (4, 4, 4, 2)):
+        step = step if sign > 0 else (size - step) % size
+        moved.append(lax.rem(at + step, size) if step else at)
+    return tuple(moved)
+
+
+def moe_kernel(
+    residual,
+    summed,
+    gain,
+    index,
+    weights,
+    slot_of,
+    gate,
+    up,
+    down,
+    shared_gate,
+    shared_up,
+    shared_down,
+    out,
+    sent,
+    arrived,
+    back,
+    returned,
+    gate_v,
+    up_v,
+    down_v,
+    shared_gate_v,
+    shared_up_v,
+    shared_down_v,
+    rows_,
+    hidden,
+    match_high,
+    match_low,
+    base,
+    load_sem,
+    out_send,
+    out_recv,
+    back_send,
+    back_recv,
+):
+    z, x, y, c = position = tuple(lax.axis_index(name) for name in ALL)
+    devices = len(MOVES)
+    loads = [
+        pltpu.make_async_copy(a, b, load_sem.at[k])
+        for k, (a, b) in enumerate(
+            (
+                (shared_gate, shared_gate_v),
+                (shared_up, shared_up_v),
+                (shared_down, shared_down_v),
+                (gate, gate_v),
+                (up, up_v),
+                (down, down_v),
+            )
+        )
+    ]
+    for load in loads:
+        load.start()
+
+    def unit(k):
+        return pl.ds(k * UNIT, UNIT)
+
+    def out_copy(k):
+        return pltpu.make_async_remote_copy(
+            src_ref=sent.at[unit(k)],
+            dst_ref=arrived.at[unit(k)],
+            send_sem=out_send.at[k],
+            recv_sem=out_recv.at[k],
+            device_id=shift(position, MOVES[k], 1),
+            device_id_type=MESH,
+        )
+
+    def back_copy(k):
+        return pltpu.make_async_remote_copy(
+            src_ref=back.at[unit(k)],
+            dst_ref=returned.at[unit(k)],
+            send_sem=back_send.at[k],
+            recv_sem=back_recv.at[k],
+            device_id=shift(position, MOVES[k], -1),
+            device_id_type=MESH,
+        )
+
+    total = (residual[...].astype(F32) + summed[...]).astype(BF16)
+    wide = total.astype(F32)
+    mean = jnp.mean(wide * wide, axis=-1, keepdims=True)
+    normed = (wide * lax.rsqrt(mean + NORM_EPSILON) * gain[...]).astype(BF16)
+    base[...] = wide
+    rows, width = normed.shape
+    part = width // PARTS
+    stacked = jnp.concatenate([normed[:, q * part : (q + 1) * part] for q in range(PARTS)], axis=0)
+
+    ids = index[...]
+    relative = (
+        ((((ids >> 5) - z) & 3) << 5)
+        + ((((ids >> 3) - x) & 3) << 3)
+        + ((((ids >> 1) - y) & 3) << 1)
+        + ((ids - c) & 1)
+    )
+    lanes = iota((rows, LANES), 1)
     chosen = jnp.zeros((rows, LANES), F32)
-    for k in range(top):
-        chosen += jnp.where(index[:, k : k + 1] == experts, 1.0, 0.0)
+    scale = jnp.zeros((rows, LANES), F32)
+    for k in range(ids.shape[1]):
+        here = relative[:, k : k + 1] == lanes
+        chosen += jnp.where(here, 1.0, 0.0)
+        scale += jnp.where(here, weights[:, k : k + 1], 0.0)
+    chosen = nn(chosen.astype(BF16), slot_of[...])
+    high, low = [nn(half, slot_of[...]).astype(BF16) for half in halves(scale)]
     earlier = jnp.where(iota((rows, rows), 0) > iota((rows, rows), 1), 1.0, 0.0).astype(BF16)
     rank = nn(earlier, chosen.astype(BF16))
-    code = (chosen * (rank + 1.0)).astype(BF16)
-    return jnp.concatenate([code] * PARTS, axis=0)
-
-
-def dispatch_kernel(residual, summed, gain, index, attended, normed, sent):
-    total = (residual[...].astype(F32) + summed[...]).astype(BF16)
-    attended[...] = total
-    wide = total.astype(F32)
-    mean = jnp.mean(wide * wide, axis=-1, keepdims=True)
-    rows_ = (wide * lax.rsqrt(mean + NORM_EPSILON) * gain[...]).astype(BF16)
-    normed[...] = rows_
-    rows, width = rows_.shape
-    part = width // PARTS
-    stacked = jnp.concatenate([rows_[:, q * part : (q + 1) * part] for q in range(PARTS)], axis=0)
-    code = routing(index)
-    shape = (256, PARTS * rows)
+    code = jnp.concatenate([(chosen * (rank + 1.0)).astype(BF16)] * PARTS, axis=0)
+    high, low = [jnp.concatenate([half] * PARTS, axis=0) for half in (high, low)]
+
+    groups = sent.shape[0] // GROUP
+    per = GROUP // UNIT
+    shape = (GROUP, PARTS * rows)
     place = iota(shape, 0) % UNIT
     fits = (place // SLOTS) == (iota(shape, 1) // rows)
     wanted = (place % SLOTS + 1).astype(F32)
-    for k in range(sent.shape[0] // 256):
-        select = (iota((256, LANES), 0) + 256 * k) // UNIT == iota((256, LANES), 1)
-        found = nt(jnp.where(select, 1.0, 0.0).astype(BF16), code)
+
+    def select(k):
+        found = (iota((GROUP, LANES), 0) + GROUP * k) // UNIT == iota((GROUP, LANES), 1)
+        return jnp.where(found, 1.0, 0.0).astype(BF16)
+
+    def launch(k):
+        for slot in range(per * k, min(per * (k + 1), devices - 1)):
+            out_copy(slot).start()
+
+    for k in range(groups):
+        found = nt(select(k), code)
         taken = jnp.where(fits & (found == wanted), 1.0, 0.0).astype(BF16)
-        sent[256 * k : 256 * (k + 1), :] = nn(taken, stacked).astype(BF16)
-
-
-def dispatch_call(residual, summed, gain, index, devices):
-    rows, width = residual.shape
-    return pl.pallas_call(
-        dispatch_kernel,
-        out_shape=[
-            jax.ShapeDtypeStruct((rows, width), BF16),
-            jax.ShapeDtypeStruct((rows, width), BF16),
-            jax.ShapeDtypeStruct((devices * UNIT, width // PARTS), BF16),
-        ],
-        in_specs=whole(4),
-        out_specs=whole(3),
-        name="dispatch",
-    )(residual, summed, gain, index)
-
-
-def expert_kernel(arrived, gate, up, down, out, rows_, hidden):
-    part = arrived.shape[1]
-    groups = arrived.shape[0] // 256
-    a, b = iota((256, 256), 0), iota((256, 256), 1)
+        sent[GROUP * k : GROUP * (k + 1), :] = nn(taken, stacked).astype(BF16)
+        if k:
+            launch(k - 1)
+    launch(groups - 1)
+    arrived[unit(devices - 1), :] = sent[unit(devices - 1), :]
+
+    for load in loads[:2]:
+        load.wait()
+    gate_val = nn(normed, shared_gate_v[...])
+    up_val = nn(normed, shared_up_v[...])
+    shared = (gate_val * jax.nn.sigmoid(gate_val) * up_val).astype(BF16)
+    loads[2].wait()
+    for at in range(0, width, 512):
+        base[:, at : at + 512] += nn(shared, shared_down_v[:, at : at + 512])
+
+    shape = (PARTS * rows, GROUP)
+    place = iota(shape, 1) % UNIT
+    fits = (place // SLOTS) == (iota(shape, 0) // rows)
+    wanted = (place % SLOTS + 1).astype(F32)
+    for k in range(groups):
+        chosen_here = select(k)
+        match = fits & (nt(code, chosen_here) == wanted)
+        match_high[k] = jnp.where(match, nt(high, chosen_here), 0.0).astype(BF16)
+        match_low[k] = jnp.where(match, nt(low, chosen_here), 0.0).astype(BF16)
+
+    a, b = iota((GROUP, GROUP), 0), iota((GROUP, GROUP), 1)
     here = (b % UNIT // SLOTS) * 64 + (b // UNIT) * SLOTS + b % SLOTS
     order = jnp.where(a == here, 1.0, 0.0).astype(BF16)
     there = (a % UNIT // SLOTS) * 64 + (a // UNIT) * SLOTS + a % SLOTS
-    back = jnp.where(b == there, 1.0, 0.0).astype(BF16)
+    order_back = jnp.where(b == there, 1.0, 0.0).astype(BF16)
+    for load in loads[3:]:
+        load.wait()
+
+    span = groups // CHUNKS
+
+    def reply(k):
+        for slot in range(per * span * k, min(per * span * (k + 1), devices - 1)):
+            back_copy(slot).start()
+
+    for chunk in range(CHUNKS):
+        for slot in range(per * span * chunk, min(per * span * (chunk + 1), devices - 1)):
+            out_copy(slot).wait_recv()
+        for g in range(span):
+            k = chunk * span + g
+            sorted_ = nn(order, arrived[GROUP * k : GROUP * (k + 1), :]).astype(BF16)
+            for q in range(PARTS):
+                rows_[64 * g : 64 * (g + 1), q * part : (q + 1) * part] = sorted_[
+                    64 * q : 64 * (q + 1)
+                ]
+        for at in range(0, hidden.shape[1], 256):
+            gate_val = nn(rows_[...], gate_v[:, at : at + 256])
+            up_val = nn(rows_[...], up_v[:, at : at + 256])
+            hidden[:, at : at + 256] = (gate_val * jax.nn.sigmoid(gate_val) * up_val).astype(BF16)
+        for at in range(0, width, 512):
+            rows_[:, at : at + 512] = nn(hidden[...], down_v[:, at : at + 512]).astype(BF16)
+        for g in range(span):
+            k = chunk * span + g
+            gathered = jnp.concatenate(
+                [rows_[64 * g : 64 * (g + 1), q * part : (q + 1) * part] for q in range(PARTS)],
+                axis=0,
+            )
+            back[GROUP * k : GROUP * (k + 1), :] = nn(order_back, gathered).astype(BF16)
+        reply(chunk)
+    returned[unit(devices - 1), :] = back[unit(devices - 1), :]
+
+    routed = jnp.zeros((PARTS * rows, part), F32)
     for k in range(groups):
-        sorted_ = nn(order, arrived[256 * k : 256 * (k + 1), :]).astype(BF16)
-        for q in range(PARTS):
-            rows_[64 * k : 64 * (k + 1), q * part : (q + 1) * part] = sorted_[64 * q : 64 * (q + 1)]
-    for at in range(0, hidden.shape[1], 256):
-        gate_val = nn(rows_[...], gate[:, at : at + 256])
-        up_val = nn(rows_[...], up[:, at : at + 256])
-        hidden[:, at : at + 256] = (gate_val * jax.nn.sigmoid(gate_val) * up_val).astype(BF16)
-    for at in range(0, rows_.shape[1], 512):
-        rows_[:, at : at + 512] = nn(hidden[...], down[:, at : at + 512]).astype(BF16)
-    for k in range(groups):
-        stacked = jnp.concatenate(
-            [rows_[64 * k : 64 * (k + 1), q * part : (q + 1) * part] for q in range(PARTS)], axis=0
-        )
-        out[256 * k : 256 * (k + 1), :] = nn(back, stacked).astype(BF16)
-
-
-def expert_call(arrived, gate, up, down):
-    slots = arrived.shape[0] // PARTS
-    return pl.pallas_call(
-        expert_kernel,
-        out_shape=jax.ShapeDtypeStruct(arrived.shape, BF16),
-        in_specs=whole(4),
-        out_specs=whole(1)[0],
-        scratch_shapes=[
-            pltpu.VMEM((slots, gate.shape[0]), BF16),
-            pltpu.VMEM((slots, gate.shape[1]), BF16),
-        ],
-        compiler_params=pltpu.CompilerParams(vmem_limit_bytes=60 * 1024 * 1024),
-        name="expert",
-    )(arrived, gate, up, down)
-
-
-def combine_kernel(attended, shared, returned, index, weights, out):
-    rows, width = attended.shape
-    part = width // PARTS
-    code = routing(index)
-    experts = iota((rows, LANES), 1)
-    scale = jnp.zeros((rows, LANES), F32)
-    for k in range(index.shape[1]):
-        scale += jnp.where(index[:, k : k + 1] == experts, weights[:, k : k + 1], 0.0)
-    high, low = halves(jnp.concatenate([scale] * PARTS, axis=0))
-    shape = (PARTS * rows, 256)
-    place = iota(shape, 1) % UNIT
-    fits = (place // SLOTS) == (iota(shape, 0) // rows)
-    wanted = (place % SLOTS + 1).astype(F32)
-    routed = jnp.zeros((PARTS * rows, part), F32)
-    for k in range(returned.shape[0] // 256):
-        select = (iota((256, LANES), 0) + 256 * k) // UNIT == iota((256, LANES), 1)
-        select = jnp.where(select, 1.0, 0.0).astype(BF16)
-        match = fits & (nt(code, select) == wanted)
-        block = returned[256 * k : 256 * (k + 1), :]
-        routed += nn(jnp.where(match, nt(high, select), 0.0).astype(BF16), block)
-        routed += nn(jnp.where(match, nt(low, select), 0.0).astype(BF16), block)
+        for slot in range(per * k, min(per * (k + 1), devices - 1)):
+            back_copy(slot).wait_recv()
+        block = returned[GROUP * k : GROUP * (k + 1), :]
+        routed += nn(match_high[k], block) + nn(match_low[k], block)
     for q in range(PARTS):
         at = slice(q * part, (q + 1) * part)
-        out[:, at] = (
-            attended[:, at].astype(F32) + shared[:, at] + routed[q * rows : (q + 1) * rows, :]
-        ).astype(BF16)
-
-
-def combine_call(attended, shared, returned, index, weights):
+        out[:, at] = (base[:, at] + routed[q * rows : (q + 1) * rows, :]).astype(BF16)
+    for slot in range(devices - 1):
+        out_copy(slot).wait_send()
+        back_copy(slot).wait_send()
+
+
+def moe_call(residual, summed, gain, index, weights, gate, up, down, *shared):
+    rows, width = residual.shape
+    devices = len(MOVES)
+    slot_of = np.zeros((devices, devices), np.float32)
+    for slot, (dz, dx, dy, dc) in enumerate(MOVES):
+        slot_of[((dz * 4 + dx) * 4 + dy) * 2 + dc, slot] = 1.0
+    slots = pltpu.VMEM((devices * UNIT, width // PARTS), BF16)
+    groups = devices * UNIT // GROUP
+    match = pltpu.VMEM((groups, PARTS * rows, GROUP), BF16)
+    chunk_rows = devices * SLOTS // CHUNKS
     return pl.pallas_call(
-        combine_kernel,
-        out_shape=jax.ShapeDtypeStruct(attended.shape, BF16),
-        in_specs=whole(5),
+        moe_kernel,
+        out_shape=jax.ShapeDtypeStruct((rows, width), BF16),
+        in_specs=whole(6) + [pl.BlockSpec(memory_space=pl.ANY)] * 6,
         out_specs=whole(1)[0],
-        name="combine",
-    )(attended, shared, returned, index, weights)
-
-
-def swap_kernel(source, out, send, recv, own_sem):
-    z, x, y, c = [lax.axis_index(name) for name in ALL]
-    me = ((z * 4 + x) * 4 + y) * 2 + c
-    devices = source.shape[0] // UNIT
-
-    def block(k):
-        return pl.ds(pl.multiple_of(k * UNIT, UNIT), UNIT)
-
-    def copy(d):
-        dz, dx, dy, dc = d % 4, d // 4 % 4, d // 16 % 4, d // 64
-        pz, px, py, pc = (z + dz) % 4, (x + dx) % 4, (y + dy) % 4, (c + dc) % 2
-        peer = ((pz * 4 + px) * 4 + py) * 2 + pc
-        sz, sx, sy, sc = (z - dz + 4) % 4, (x - dx + 4) % 4, (y - dy + 4) % 4, (c - dc + 2) % 2
-        giver = ((sz * 4 + sx) * 4 + sy) * 2 + sc
-        start = pltpu.make_async_remote_copy(
-            src_ref=source.at[block(peer)],
-            dst_ref=out.at[block(me)],
-            send_sem=send.at[d],
-            recv_sem=recv.at[d],
-            device_id=(pz, px, py, pc),
-            device_id_type=MESH,
-        )
-        arrive = pltpu.make_async_remote_copy(
-            src_ref=source.at[block(peer)],
-            dst_ref=out.at[block(giver)],
-            send_sem=send.at[d],
-            recv_sem=recv.at[d],
-            device_id=(pz, px, py, pc),
-            device_id_type=MESH,
-        )
-        return start, arrive
-
-    @pl.loop(1, devices)
-    def _(d):
-        copy(d)[0].start()
-
-    out[block(me), :] = source[block(me), :]
-
-    @pl.loop(1, devices)
-    def _(d):
-        copy(d)[1].wait()
-
-
-def swap_call(source):
-    devices = source.shape[0] // UNIT
-    return pl.pallas_call(
-        swap_kernel,
-        out_shape=jax.ShapeDtypeStruct(source.shape, BF16),
-        in_specs=whole(1),
-        out_specs=whole(1)[0],
-        scratch_shapes=[pltpu.SemaphoreType.DMA((devices,))] * 2 + [pltpu.SemaphoreType.DMA],
-        compiler_params=pltpu.CompilerParams(has_side_effects=True),
-        name="swap",
-    )(source)
-
-
-def swiglu_hidden(inputs, w_gate, w_up):
-    gate_val = jnp.dot(inputs, w_gate, preferred_element_type=F32)
-    up_val = jnp.dot(inputs, w_up, preferred_element_type=F32)
-    return (jax.nn.silu(gate_val) * up_val).astype(BF16)
-
-
-def exchange_slots(slots):
-    devices = slots.shape[0] // UNIT
-    return lax.all_to_all(
-        slots.reshape(devices, UNIT, -1), ALL, split_axis=0, concat_axis=0, tiled=True
-    ).reshape(slots.shape)
+        scratch_shapes=[slots] * 4
+        + [pltpu.VMEM(a.shape, BF16) for a in (gate, up, down, *shared)]
+        + [
+            pltpu.VMEM((chunk_rows, width), BF16),
+            pltpu.VMEM((chunk_rows, gate.shape[1]), BF16),
+            match,
+            match,
+            pltpu.VMEM((rows, width), F32),
+            pltpu.SemaphoreType.DMA((6,)),
+        ]
+        + [pltpu.SemaphoreType.DMA((devices,))] * 4,
+        compiler_params=pltpu.CompilerParams(
+            has_side_effects=True, vmem_limit_bytes=48 * 1024 * 1024
+        ),
+        name="experts",
+    )(residual, summed, gain, index, weights, jnp.asarray(slot_of, BF16), gate, up, down, *shared)
 
 
 def local(
@@ -686,21 +745,19 @@
         width,
     )
     summed = scatter_call(partial.reshape(-1, residual.shape[0], width))
-    devices = lax.axis_size(ALL)
-    attended, normed, slots = dispatch_call(
-        residual, summed, feedforward_gain[None, :], routed_expert_index, devices
+    return moe_call(
+        residual,
+        summed,
+        feedforward_gain[None, :],
+        routed_expert_index,
+        routed_expert_weight,
+        expert_gate_weight[0],
+        expert_up_weight[0],
+        expert_down_weight[0],
+        shared_gate_weight,
+        shared_up_weight,
+        shared_down_weight,
     )
-    arrived = exchange_slots(slots)
-    result = expert_call(
-        arrived, expert_gate_weight[0], expert_up_weight[0], expert_down_weight[0]
-    )
-    returned = exchange_slots(result)
-    shared_out = jnp.dot(
-        swiglu_hidden(normed, shared_gate_weight, shared_up_weight),
-        shared_down_weight,
-        preferred_element_type=F32,
-    )
-    return combine_call(attended, shared_out, returned, routed_expert_index, routed_expert_weight)
 
 
 def solution(mesh):

time: 148 us -> 125 us (0.84)
  Pallas kernels: 71.7 us -> 119 us
  blocking collectives: 37.8 us -> 0 us
  waiting for transfers between devices: 23.8 us -> 0 us
  starting transfers between devices: 6.11 us -> 0 us
  matrix products: 5.37 us -> 0 us
    pallas_call x3 -> x1, Pallas kernels: 20.1 us -> 67.4 us  [moe_call(): pl.pallas_call(moe_kernel, out_shape=jax.ShapeDtypeStruct((rows, width),...]
    all_to_all x1 -> x0, blocking collectives: 37.8 us -> none  [exchange_slots(): lax.all_to_all(slots.reshape(devices, UNIT, -1), ALL, split_axis=0, conca...]
    all_to_all x1 -> x0, waiting for transfers between devices: 23.8 us -> none  [exchange_slots(): lax.all_to_all(slots.reshape(devices, UNIT, -1), ALL, split_axis=0, conca...]
    all_to_all x1 -> x0, starting transfers between devices: 6.11 us -> none  [exchange_slots(): lax.all_to_all(slots.reshape(devices, UNIT, -1), ALL, split_axis=0, conca...]
    dot_general x2 -> x0, matrix products: 5.37 us -> none  [the longest x1 3.31 us: local(): jnp.dot(swiglu_hidden(normed, shared_gate_weight, shared_up_weight), shar...]
    unnamed x8 -> x19, local copies, waits for them, and re-layouts: 2.22 us -> 3.55 us
  transfers between devices with their start and end apart: 1 -> 0, of which waited for: 1 -> 0; matrix products, arithmetic and copies ran while one was open for 4% -> 0% of each run, Pallas kernels for 0% -> 0%
where the time goes in v1:
time: 125 us; the launch traced here: 123 us
  Pallas kernels  119 us (95%)
  local copies, waits for them, and re-layouts  3.55 us (3%)
    pallas_call x1, Pallas kernels, moe_call(): pl.pallas_call(moe_kernel, out_shape=jax.ShapeDtypeStruct((rows, width),...  67.4 us
    pallas_call x1, Pallas kernels, scatter_call(): pl.pallas_call(scatter_kernel, out_shape=jax.ShapeDtypeStruct((rows, widt...  21.6 us
    pallas_call x1, Pallas kernels, exchange_call(): pl.pallas_call(exchange_kernel, out_shape=[shape, shape], in_specs=whole(...  18.7 us
    pallas_call x1, Pallas kernels, local_call(): pl.pallas_call(functools.partial(local_kernel, dot), out_shape=shapes, in...  6.99 us
    pallas_call x1, Pallas kernels, project_call(): pl.pallas_call(project_kernel, out_shape=jax.ShapeDtypeStruct((rows, widt...  4.51 us
    unnamed x19, local copies, waits for them, and re-layouts  3.55 us

profile of v1, /device:TPU:1, one launch (start us, length us, event | category | flops | bytes accessed | tf_op | source)
XLA Modules:
  0.0 122.8 jit_solution(6417295826670694806)
XLA Ops:
  0.0 7.0 %local_terms.1 = (f32[512,128]{1,0:T(8,128)}, bf16[512,128]{1,0:T(8,128)(2,1)}, f32[512,128]{1,0:T(8,128)}, bf16[512,128]{1,0:T(8,128)(2,1)}, bf16[192,256]{1,0:T(8,128)(2,1)}) custom-call(bf16[512,128]{1,0:T(8,128)(2,1)} %refs_0_.1, bf16[512,128]{1,0:T(8,128)(2,1)} %refs_1_.1, bf16[512,128]{1,0:T(8,128)(2,1)} %refs_2_.1, bf16[512,128]{1,0:T(8,128)(2,1)} %refs_3_.1, ...), custom_call_target="tpu_custom_call" | custom-call | tf_op jit(solution)/shard_map/local_terms/pallas_call | solution.py:190
  7.0 18.7 %exchange.1 = (f32[128,128]{1,0:T(8,128)}, f32[128,128]{1,0:T(8,128)}) custom-call(bf16[192,256]{1,0:T(8,128)(2,1)} %get-tuple-element.14.message), custom_call_target="tpu_custom_call" | custom-call | tf_op jit(solution)/shard_map/exchange/pallas_call | solution.py:317
  25.7 4.5 %project.1 = bf16[512,2048]{1,0:T(8,128)(2,1)} custom-call(f32[512,128]{1,0:T(8,128)} %get-tuple-element.12.read_a, bf16[512,128]{1,0:T(8,128)(2,1)} %get-tuple-element.13.map_a, f32[128,128]{1,0:T(8,128)} %get-tuple-element.15.enter_a, f32[1,128]{1,0:T(1,128)} %bitcast.18, bf16[128,2048]{1,0:T(8,128)(2,1)} %weight_a.1, ...), custom_call_target="tpu_custom_call" | custom-call | tf_op jit(solution)/shard_map/project/pallas_call | solution.py:359
  30.2 0.0 copy-start.6
  30.2 0.0 copy-start.7
  30.2 0.0 copy-start.1
  30.2 0.0 copy-start.3
  30.3 0.0 copy-start.4
  30.3 0.0 copy-start.5
  30.3 21.6 %scatter_sum.1.summed = f32[64,2048]{1,0:T(8,128)} custom-call(bf16[8,64,2048]{2,1,0:T(8,128)(2,1)} %bitcast.13), custom_call_target="tpu_custom_call" | custom-call | tf_op jit(solution)/shard_map/scatter_sum/pallas_call | solution.py:412
  51.9 0.0 copy-done.6
  51.9 0.1 copy.29.index
  52.0 0.0 copy-done.7
  52.0 0.1 copy.30.weights
  52.1 0.0 copy-done.1
  52.1 0.0 copy-done.3
  52.1 0.0 copy-done.4
  52.1 0.0 copy-done.5
  52.1 0.0 copy-start
  52.1 1.0 copy-done
  53.2 0.0 copy-start.2
  53.2 1.6 %copy-done.2 = bf16[1,2048,512]{2,1,0:T(8,128)(2,1)S(1)} copy-done((bf16[1,2048,512]{2,1,0:T(8,128)(2,1)S(1)}, bf16[1,2048,512]{2,1,0:T(8,128)(2,1)}, u32[]{:S(2)}) %copy-start.2) | copy-done | bytes 2097176
  54.7 67.4 %experts.1 = bf16[64,2048]{1,0:T(8,128)(2,1)S(1)} custom-call(bf16[64,2048]{1,0:T(8,128)(2,1)S(1)} %copy-done.3, f32[64,2048]{1,0:T(8,128)S(1)} %copy-done, f32[1,2048]{1,0:T(1,128)S(1)} %bitcast.12, s32[64,4]{1,0:T(8,128)S(1)} %copy.29.index, f32[64,4]{1,0:T(8,128)S(1)} %copy.30.weights, bf16[128,128]{1,0:T(8,128)(2,1)S(1)} %copy-done.4, ...), custom_call_target="tpu_custom_call" | custom-call | tf_op jit(solution)/shard_map/experts/pallas_call | solution.py:659
  122.1 0.7 copy.32
Async XLA Ops:
  30.2 21.6 %copy-start.6 = (s32[64,4]{0,1:T(4,128)S(1)}, s32[64,4]{0,1:T(4,128)}, u32[]{:S(2)}) copy-start(s32[64,4]{0,1:T(4,128)} %param.47) | copy-start | bytes 3076
  30.2 21.7 %copy-start.7 = (f32[64,4]{0,1:T(4,128)S(1)}, f32[64,4]{0,1:T(4,128)}, u32[]{:S(2)}) copy-start(f32[64,4]{0,1:T(4,128)} %param.48) | copy-start | bytes 3076
  30.2 21.8 %copy-start.1 = (bf16[1,2048,512]{2,1,0:T(8,128)(2,1)S(1)}, bf16[1,2048,512]{2,1,0:T(8,128)(2,1)}, u32[]{:S(2)}) copy-start(bf16[1,2048,512]{2,1,0:T(8,128)(2,1)} %param.49) | copy-start | bytes 6291460
  30.2 21.8 %copy-start.3 = (bf16[64,2048]{1,0:T(8,128)(2,1)S(1)}, bf16[64,2048]{1,0:T(8,128)(2,1)}, u32[]{:S(2)}) copy-start(bf16[64,2048]{1,0:T(8,128)(2,1)} %residual.1) | copy-start | bytes 786436
  30.3 21.8 %copy-start.4 = (bf16[128,128]{1,0:T(8,128)(2,1)S(1)}, bf16[128,128]{1,0:T(8,128)(2,1)}, u32[]{:S(2)}) copy-start(bf16[128,128]{1,0:T(8,128)(2,1)} %constant.2.clone.slot_of) | copy-start | bytes 98308
  30.3 21.8 %copy-start.5 = (f32[2048]{0:T(1024)S(1)}, f32[2048]{0:T(1024)}, u32[]{:S(2)}) copy-start(f32[2048]{0:T(1024)} %param.46) | copy-start | bytes 24580
  52.1 1.0 copy-start
  53.2 1.6 %copy-start.2 = (bf16[1,2048,512]{2,1,0:T(8,128)(2,1)S(1)}, bf16[1,2048,512]{2,1,0:T(8,128)(2,1)}, u32[]{:S(2)}) copy-start(bf16[1,2048,512]{2,1,0:T(8,128)(2,1)} %param.50) | copy-start | bytes 6291460

commit v2 on v1

v2 whole, which is shorter than its diff:
```python
import functools
import itertools

import jax
import jax.numpy as jnp
import numpy as np
from jax import lax
from jax.experimental import pallas as pl
from jax.experimental.pallas import tpu as pltpu
from jax.sharding import Mesh
from jax.sharding import PartitionSpec as P

F32, BF16 = jnp.float32, jnp.bfloat16
SPAN = 128
LANES = 128
HEAD_SIZE_FIRST = 64
KEY_EPSILON = 1e-06
HEAD_EPSILON = 0.00064
NORM_EPSILON = 1e-06
Z, X, Y, C = "z", "x", "y", "core"
ALL = (Z, X, Y, C)
MESH = pl.DeviceIdType.MESH
SLOTS = 4
PARTS = 4
UNIT = SLOTS * PARTS
GROUP = 256
CHUNKS = 4


def distance(move):
    return sum(min(step, 4 - step) for step in move[:3])


MOVES = sorted(
    itertools.product(range(4), range(4), range(4), range(2)),
    key=lambda move: (-distance(move), -move[3]),
)


def nn(a, b):
    return lax.dot_general(a, b, (((1,), (0,)), ((), ())), preferred_element_type=F32)


def nt(a, b):
    return lax.dot_general(a, b, (((1,), (1,)), ((), ())), preferred_element_type=F32)


def halves(x):
    high = x.astype(BF16)
    return high, (x - high.astype(F32)).astype(BF16)


def dot(f, a, b):
    return f(a.astype(BF16), b.astype(BF16))


def dot3(f, a, b):
    ah, al = halves(a)
    bh, bl = halves(b)
    return f(ah, bh) + (f(ah, bl) + f(al, bh))


def iota(shape, dim):
    return lax.broadcasted_iota(jnp.int32, shape, dim)


def head_sum(x, width):
    if width == LANES:
        return jnp.sum(x, axis=-1, keepdims=True)
    lane = iota(x.shape, 1)
    left = jnp.sum(jnp.where(lane < width, x, 0.0), axis=-1, keepdims=True)
    right = jnp.sum(jnp.where(lane < width, 0.0, x), axis=-1, keepdims=True)
    return jnp.where(lane < width, left, right)


def shift(position, move, sign):
    moved = []
    for at, step, size in zip(position, move, (4, 4, 4, 2)):
        step = step if sign > 0 else (size - step) % size
        moved.append(lax.rem(at + step, size) if step else at)
    return tuple(moved)


def block_terms(groups, extra_ref):
    square = (SPAN, SPAN)
    row, col = iota(square, 0), iota(square, 1)
    lower = row >= col
    lower_bf = jnp.where(lower, 1.0, 0.0).astype(BF16)
    items = []
    for group, (r_, k_, v_, p_, c_, base_, width) in enumerate(groups):
        for block in range(r_.shape[0] // SPAN):
            at = pl.ds(block * SPAN, SPAN)
            key = k_[at, :].astype(F32)
            unit = key * lax.rsqrt(head_sum(key * key, width) + KEY_EPSILON)
            removal = unit * jax.nn.sigmoid(c_[at, :].astype(F32))
            slow = jax.nn.sigmoid(p_[at, :].astype(F32))
            extra = extra_ref[pl.ds(block, 1), :]
            rate = 2.0 * base_[...]
            high, low = halves(slow)
            run_slow = nn(lower_bf, high) + nn(lower_bf, low)
            run_extra = jnp.sum(jnp.where(lower, extra, 0.0), axis=-1, keepdims=True)
            own_extra = jnp.sum(jnp.where(row == col, extra, 0.0), axis=-1, keepdims=True)
            running = run_extra - rate * run_slow
            own_log = own_extra - rate * slow
            centre = running[SPAN // 2 - 1 : SPAN // 2, :]
            ending = running[SPAN - 1 : SPAN, :]
            grown = running - centre
            write = removal * jnp.exp(-grown)
            items.append(
                dict(
                    group=group,
                    block=block,
                    width=width,
                    read=r_[at, :].astype(F32) * jnp.exp(grown),
                    query=unit * jnp.exp(grown - own_log),
                    write=write,
                    write_end=write * jnp.exp(ending - centre),
                    value=v_[at, :].astype(F32),
                    centre=jnp.exp(centre),
                    ending=jnp.exp(ending),
                )
            )
    return items


def spread(item, x):
    if len(item["parts"]) == 1:
        return x
    first = iota(x.shape, 1) % SPAN < HEAD_SIZE_FIRST
    return jnp.concatenate([jnp.where(first, x, 0.0), jnp.where(first, 0.0, x)], axis=0)


def joined(item, name):
    return jnp.concatenate([part[name] for part in item["parts"]], axis=1)


def block_steps(items):
    square = (SPAN, SPAN)
    row, col = iota(square, 0), iota(square, 1)
    strict = row > col
    lower = row >= col
    eye = jnp.where(row == col, 1.0, 0.0)
    solves = []
    for item in items:
        lane = col < item["width"]
        masks = [None] if item["width"] == SPAN else [lane, jnp.logical_not(lane)]
        item["parts"] = []
        for mask in masks:
            query = item["query"] if mask is None else jnp.where(mask, item["query"], 0.0)
            read = item["read"] if mask is None else jnp.where(mask, item["read"], 0.0)
            both = dot(nt, jnp.concatenate([query, read], axis=0), item["write"])
            part = dict(
                coupling=jnp.where(strict, both[:SPAN], 0.0),
                reading=jnp.where(lower, both[SPAN:], 0.0),
            )
            item["parts"].append(part)
            solves.append(part)
    size = 1
    while size < SPAN:
        near = ((row // (2 * size)) == (col // (2 * size))) & ((row // size) > (col // size))
        for part in solves:
            step = jnp.where(near, part["coupling"], 0.0)
            if size == 1:
                part["inverse"] = eye - step
            else:
                inverse = part["inverse"]
                part["inverse"] = inverse - dot(nn, dot(nn, inverse, step), inverse)
        size *= 2
    same_head = (row < HEAD_SIZE_FIRST) == (col < HEAD_SIZE_FIRST)
    for item in items:
        right = jnp.concatenate([item["value"], -item["query"]], axis=1)
        solved = dot(nn, joined(item, "inverse"), spread(item, right))
        item["solved"] = solved
        scaled = jnp.concatenate([solved[:, :SPAN], solved[:, SPAN:] * item["centre"]], axis=1)
        step = dot(nn, item["write_end"].T, scaled)
        diagonal = jnp.where(row == col, item["ending"], 0.0)
        step = step + jnp.concatenate([jnp.zeros(square, F32), diagonal], axis=1)
        if item["width"] < SPAN:
            step = jnp.where(jnp.concatenate([same_head, same_head], axis=1), step, 0.0)
        item["step"] = step


def block_chain(items):
    held = None
    for item in items:
        item["held"] = held
        step = item["step"]
        if held is None:
            held = step
        else:
            held = dot(nn, step[:, SPAN:], held)
            held = jnp.concatenate([held[:, :SPAN] + step[:, :SPAN], held[:, SPAN:]], axis=1)
    return held


def block_reads(items, read_ref, map_ref):
    for item in items:
        given = dot(nn, joined(item, "reading"), spread(item, item["solved"]))
        local_read = given[:, :SPAN]
        state_read = (item["read"] + given[:, SPAN:]) * item["centre"]
        at = pl.ds(item["block"] * SPAN, SPAN)
        if item["held"] is not None:
            out = dot(nn, state_read, item["held"])
            local_read = local_read + out[:, :SPAN]
            state_read = out[:, SPAN:]
        read_ref[item["group"], at, :] = local_read
        map_ref[item["group"], at, :] = state_read.astype(BF16)


def pack(ref, first, second):
    ref[0:64, :] = (first[:64, :] + first[64:, :]).astype(BF16)
    ref[64:192, :] = second.astype(BF16)


def unpack(packed):
    square = (LANES, 2 * LANES)
    same = (iota(square, 0) < 64) == (iota(square, 1) % LANES < 64)
    top = packed[0:64, :]
    first = jnp.where(same, jnp.concatenate([top, top], axis=0), jnp.zeros((), BF16))
    return first, packed[64:192, :]


def follow(step, held):
    high, low = halves(held)
    return nn(step[:, LANES:], high) + nn(step[:, LANES:], low)


def compose(step, held):
    moved = follow(step, held)
    return jnp.concatenate(
        [moved[:, :LANES] + step[:, :LANES].astype(F32), moved[:, LANES:]], axis=1
    )


def layer_kernel(
    r_a,
    k_a,
    v_a,
    p_a,
    c_a,
    base_a,
    gain_a,
    r_b,
    k_b,
    v_b,
    p_b,
    c_b,
    base_b,
    gain_b,
    extra,
    gain,
    index,
    weights,
    slot_of,
    residual,
    weight_a,
    weight_b,
    gate,
    up,
    down,
    shared_gate,
    shared_up,
    shared_down,
    out,
    residual_v,
    weight_v,
    gate_v,
    up_v,
    down_v,
    shared_gate_v,
    shared_up_v,
    shared_down_v,
    read_v,
    map_v,
    rows_v,
    columns_v,
    message,
    total,
    enter_v,
    own,
    pair_out,
    pair_in,
    ring_out,
    ring_in,
    base,
    sent,
    arrived,
    back,
    returned,
    chunk_v,
    hidden,
    match_high,
    match_low,
    load_sem,
    row_send,
    row_recv,
    col_send,
    col_recv,
    pair_send,
    pair_recv,
    ring_send,
    ring_recv,
    out_send,
    out_recv,
    back_send,
    back_recv,
):
    z, x, y, c = position = tuple(lax.axis_index(name) for name in ALL)
    devices = len(MOVES)
    barrier = pltpu.get_barrier_semaphore()
    for move in MOVES[:-1]:
        pl.semaphore_signal(
            barrier, inc=1, device_id=shift(position, move, 1), device_id_type=MESH
        )
    pairs = (
        (weight_a, weight_v.at[pl.ds(0, LANES)]),
        (weight_b, weight_v.at[pl.ds(LANES, LANES)]),
        (residual, residual_v),
        (shared_gate, shared_gate_v),
        (shared_up, shared_up_v),
        (shared_down, shared_down_v),
        (gate, gate_v),
        (up, up_v),
        (down, down_v),
    )
    loads = [pltpu.make_async_copy(a, b, load_sem.at[k]) for k, (a, b) in enumerate(pairs)]
    for load in loads:
        load.start()

    def remote(src, dst, send, recv, goal):
        return pltpu.make_async_remote_copy(
            src_ref=src,
            dst_ref=dst,
            send_sem=send,
            recv_sem=recv,
            device_id=goal,
            device_id_type=MESH,
        )

    items = block_terms(
        (
            (r_a, k_a, v_a, p_a, c_a, base_a, HEAD_SIZE_FIRST),
            (r_b, k_b, v_b, p_b, c_b, base_b, SPAN),
        ),
        extra,
    )
    block_steps(items)
    chains = [[item for item in items if item["group"] == group] for group in range(2)]
    pack(message, *[block_chain(chain) for chain in chains])
    pl.semaphore_wait(barrier, devices - 1)

    def row_copy(d):
        goal = (z, lax.rem(x + d, 4), y, c)
        return remote(message, rows_v.at[d], row_send.at[d], row_recv.at[d], goal)

    def col_copy(d):
        goal = (lax.rem(z + d, 4), x, y, c)
        return remote(total, columns_v.at[d], col_send.at[d], col_recv.at[d], goal)

    for d in (2, 1, 3):
        row_copy(d).start()
    rows_v[0] = message[...]
    for chain in chains:
        block_reads(chain, read_v, map_v)

    square = (LANES, 2 * LANES)
    unit_step = jnp.where(iota(square, 0) + LANES == iota(square, 1), 1.0, 0.0)
    inside = [unit_step, unit_step]
    running = [unit_step, unit_step]
    for d in range(1, 4):
        row_copy(d).wait()
    for k in range(4):
        pair = unpack(rows_v[lax.rem(x - k + 4, 4)])
        inside = [jnp.where(x == k, now, old) for now, old in zip(running, inside)]
        if k == 0:
            running = [p.astype(F32) for p in pair]
        else:
            running = [compose(p, r) for p, r in zip(pair, running)]
    pack(total, *running)
    for d in (2, 1, 3):

        @pl.when(z + d < 4)
        def _():
            col_copy(d).start()

    enter_v[...] = jnp.zeros_like(enter_v)
    for k in range(3):

        @pl.when(k < z)
        def _():
            d = z - k
            remote(
                total, columns_v.at[d], col_send.at[d], col_recv.at[d], (k, x, y, c)
            ).wait_recv()
            for group, step in enumerate(unpack(columns_v[d])):
                enter_v[group] = follow(step, enter_v[group]) + step[:, :LANES].astype(F32)

    entering = []
    for group, step in enumerate(inside):
        enter = dot3(nn, step[:, LANES:], enter_v[group]) + step[:, :LANES]
        entering.append(halves(enter))

    rows, width = out.shape
    half = width // 2
    partner = (z, x, y, 1 - c)
    right, left = (z, x, lax.rem(y + 1, 4), c), (z, x, lax.rem(y + 3, 4), c)

    def pair_copy(d):
        return remote(pair_out.at[d], pair_in.at[d], pair_send.at[d], pair_recv.at[d], partner)

    def ring_copy(k):
        return remote(
            ring_out.at[k],
            ring_in.at[k],
            ring_send.at[k],
            ring_recv.at[k],
            right if k % 2 == 0 else left,
        )

    square = (LANES, LANES)
    row, col = iota(square, 0), iota(square, 1)
    for load in loads[:2]:
        load.wait()
    for d in (2, 1, 3, 0):
        start = lax.rem(y + d, 4) * (2 * rows)
        theirs = pl.ds(pl.multiple_of(start + (1 - c) * rows, rows), rows)
        mine = pl.ds(pl.multiple_of(start + c * rows, rows), rows)
        mixed = []
        for group, (head_gain, size) in enumerate(((gain_a, HEAD_SIZE_FIRST), (gain_b, SPAN))):
            mean = jnp.where((row // size) == (col // size), 1.0 / size, 0.0).astype(BF16)
            high, low = entering[group]
            maps = jnp.concatenate([map_v[group, theirs, :], map_v[group, mine, :]], axis=0)
            reads = jnp.concatenate([read_v[group, theirs, :], read_v[group, mine, :]], axis=0)
            readout = reads + nn(maps, high) + nn(maps, low)
            high, low = halves(readout)
            centred = readout - (nn(high, mean) + nn(low, mean))
            high, low = halves(centred * centred)
            variance = nn(high, mean) + nn(low, mean)
            mixed.append((centred * lax.rsqrt(variance + HEAD_EPSILON) * head_gain[...]).astype(BF16))
        both = jnp.concatenate(mixed, axis=1)
        for at in range(0, width, 512):
            product = nn(both, weight_v[:, at : at + 512])
            pair_out[d, :, at : at + 512] = product[:rows].astype(BF16)
            own[d, :, at : at + 512] = product[rows:]
        pair_copy(d).start()

    pair_copy(2).wait()
    for k in range(2):
        at = slice(k * half, (k + 1) * half)
        ring_out[k] = (own[2, :, at] + pair_in[2, :, at].astype(F32)).astype(BF16)
    for k in range(2):
        ring_copy(k).start()
    for k, d, at, keep in (
        (2, 1, slice(half, width), slice(0, half)),
        (3, 3, slice(0, half), slice(half, width)),
    ):
        pair_copy(d).wait()
        ring_out[k] = (own[d, :, at] + pair_in[d, :, at].astype(F32)).astype(BF16)
        ring_copy(k).start()
        own[d, :, keep] += pair_in[d, :, keep].astype(F32)
    pair_copy(0).wait()
    loads[2].wait()
    base[...] = residual_v[...].astype(F32) + (own[0] + pair_in[0].astype(F32))
    for k, d, keep in ((4, 1, slice(0, half)), (5, 3, slice(half, width))):
        ring_copy(k - 4).wait()
        ring_out[k] = (own[d, :, keep] + ring_in[k - 4].astype(F32)).astype(BF16)
        ring_copy(k).start()
    for k, at in (
        (2, slice(half, width)),
        (3, slice(0, half)),
        (4, slice(0, half)),
        (5, slice(half, width)),
    ):
        ring_copy(k).wait()
        base[:, at] += ring_in[k].astype(F32)

    def unit(k):
        return pl.ds(k * UNIT, UNIT)

    def out_copy(k):
        return remote(
            sent.at[unit(k)],
            arrived.at[unit(k)],
            out_send.at[k],
            out_recv.at[k],
            shift(position, MOVES[k], 1),
        )

    def back_copy(k):
        return remote(
            back.at[unit(k)],
            returned.at[unit(k)],
            back_send.at[k],
            back_recv.at[k],
            shift(position, MOVES[k], -1),
        )

    wide = base[...].astype(BF16).astype(F32)
    mean = jnp.mean(wide * wide, axis=-1, keepdims=True)
    normed = (wide * lax.rsqrt(mean + NORM_EPSILON) * gain[...]).astype(BF16)
    base[...] = wide
    part = width // PARTS
    stacked = jnp.concatenate([normed[:, q * part : (q + 1) * part] for q in range(PARTS)], axis=0)

    ids = index[...]
    relative = (
        ((((ids >> 5) - z) & 3) << 5)
        + ((((ids >> 3) - x) & 3) << 3)
        + ((((ids >> 1) - y) & 3) << 1)
        + ((ids - c) & 1)
    )
    experts = iota((LANES, rows), 0)
    chosen = jnp.zeros((LANES, rows), F32)
    scale = jnp.zeros((LANES, rows), F32)
    for k in range(ids.shape[0]):
        here = relative[k : k + 1, :] == experts
        chosen += jnp.where(here, 1.0, 0.0)
        scale += jnp.where(here, weights[k : k + 1, :], 0.0)
    chosen = nn(chosen.T.astype(BF16), slot_of[...])
    high, low = [nn(term, slot_of[...]).astype(BF16) for term in halves(scale.T)]
    earlier = jnp.where(iota((rows, rows), 0) > iota((rows, rows), 1), 1.0, 0.0).astype(BF16)
    rank = nn(earlier, chosen.astype(BF16))
    code = jnp.concatenate([(chosen * (rank + 1.0)).astype(BF16)] * PARTS, axis=0)
    high, low = [jnp.concatenate([term] * PARTS, axis=0) for term in (high, low)]

    groups = sent.shape[0] // GROUP
    per = GROUP // UNIT
    shape = (GROUP, PARTS * rows)
    place = iota(shape, 0) % UNIT
    fits = (place // SLOTS) == (iota(shape, 1) // rows)
    wanted = (place % SLOTS + 1).astype(F32)

    def select(k):
        found = (iota((GROUP, LANES), 0) + GROUP * k) // UNIT == iota((GROUP, LANES), 1)
        return jnp.where(found, 1.0, 0.0).astype(BF16)

    def launch(k):
        for slot in range(per * k, min(per * (k + 1), devices - 1)):
            out_copy(slot).start()

    for k in range(groups):
        found = nt(select(k), code)
        taken = jnp.where(fits & (found == wanted), 1.0, 0.0).astype(BF16)
        sent[GROUP * k : GROUP * (k + 1), :] = nn(taken, stacked).astype(BF16)
        if k:
            launch(k - 1)
    launch(groups - 1)
    arrived[unit(devices - 1), :] = sent[unit(devices - 1), :]

    for load in loads[3:5]:
        load.wait()
    gate_val = nn(normed, shared_gate_v[...])
    up_val = nn(normed, shared_up_v[...])
    shared = (gate_val * jax.nn.sigmoid(gate_val) * up_val).astype(BF16)
    loads[5].wait()
    for at in range(0, width, 512):
        base[:, at : at + 512] += nn(shared, shared_down_v[:, at : at + 512])

    shape = (PARTS * rows, GROUP)
    place = iota(shape, 1) % UNIT
    fits = (place // SLOTS) == (iota(shape, 0) // rows)
    wanted = (place % SLOTS + 1).astype(F32)
    for k in range(groups):
        chosen_here = select(k)
        match = fits & (nt(code, chosen_here) == wanted)
        match_high[k] = jnp.where(match, nt(high, chosen_here), 0.0).astype(BF16)
        match_low[k] = jnp.where(match, nt(low, chosen_here), 0.0).astype(BF16)

    a, b = iota((GROUP, GROUP), 0), iota((GROUP, GROUP), 1)
    here = (b % UNIT // SLOTS) * 64 + (b // UNIT) * SLOTS + b % SLOTS
    order = jnp.where(a == here, 1.0, 0.0).astype(BF16)
    there = (a % UNIT // SLOTS) * 64 + (a // UNIT) * SLOTS + a % SLOTS
    order_back = jnp.where(b == there, 1.0, 0.0).astype(BF16)
    for load in loads[6:]:
        load.wait()

    span = groups // CHUNKS

    def chunk_slots(k):
        return range(per * span * k, min(per * span * (k + 1), devices - 1))

    for chunk in range(CHUNKS):
        for slot in chunk_slots(chunk):
            out_copy(slot).wait_recv()
        for g in range(span):
            k = chunk * span + g
            sorted_ = nn(order, arrived[GROUP * k : GROUP * (k + 1), :]).astype(BF16)
            for q in range(PARTS):
                chunk_v[64 * g : 64 * (g + 1), q * part : (q + 1) * part] = sorted_[
                    64 * q : 64 * (q + 1)
                ]
        for at in range(0, hidden.shape[1], 256):
            gate_val = nn(chunk_v[...], gate_v[:, at : at + 256])
            up_val = nn(chunk_v[...], up_v[:, at : at + 256])
            hidden[:, at : at + 256] = (gate_val * jax.nn.sigmoid(gate_val) * up_val).astype(BF16)
        for at in range(0, width, 512):
            chunk_v[:, at : at + 512] = nn(hidden[...], down_v[:, at : at + 512]).astype(BF16)
        for g in range(span):
            k = chunk * span + g
            gathered = jnp.concatenate(
                [chunk_v[64 * g : 64 * (g + 1), q * part : (q + 1) * part] for q in range(PARTS)],
                axis=0,
            )
            back[GROUP * k : GROUP * (k + 1), :] = nn(order_back, gathered).astype(BF16)
        for slot in chunk_slots(chunk):
            back_copy(slot).start()
    returned[unit(devices - 1), :] = back[unit(devices - 1), :]

    routed = jnp.zeros((PARTS * rows, part), F32)
    for k in range(groups):
        for slot in range(per * k, min(per * (k + 1), devices - 1)):
            back_copy(slot).wait_recv()
        block = returned[GROUP * k : GROUP * (k + 1), :]
        routed += nn(match_high[k], block) + nn(match_low[k], block)
    for q in range(PARTS):
        at = slice(q * part, (q + 1) * part)
        out[:, at] = (base[:, at] + routed[q * rows : (q + 1) * rows, :]).astype(BF16)
    for d in (2, 1, 3):

        @pl.when(z + d < 4)
        def _():
            col_copy(d).wait_send()

    for slot in range(devices - 1):
        out_copy(slot).wait_send()
        back_copy(slot).wait_send()


def slot_table():
    devices = len(MOVES)
    table = np.zeros((devices, devices), np.float32)
    for slot, (dz, dx, dy, dc) in enumerate(MOVES):
        table[((dz * 4 + dx) * 4 + dy) * 2 + dc, slot] = 1.0
    return jnp.asarray(table, BF16)


def layer_call(small, large):
    rows, width = large[0].shape
    long = small[0].shape[0]
    gate = large[3]
    devices = len(MOVES)
    part = width // PARTS
    slots = pltpu.VMEM((devices * UNIT, part), BF16)
    match = pltpu.VMEM((devices * UNIT // GROUP, PARTS * rows, GROUP), BF16)
    chunk_rows = devices * SLOTS // CHUNKS
    packed = (192, 2 * LANES)
    scratch = (
        [pltpu.VMEM((rows, width), BF16), pltpu.VMEM((2 * LANES, width), BF16)]
        + [pltpu.VMEM(a.shape, BF16) for a in large[3:]]
        + [
            pltpu.VMEM((2, long, LANES), F32),
            pltpu.VMEM((2, long, LANES), BF16),
            pltpu.VMEM((4, *packed), BF16),
            pltpu.VMEM((4, *packed), BF16),
            pltpu.VMEM(packed, BF16),
            pltpu.VMEM(packed, BF16),
            pltpu.VMEM((2, LANES, LANES), F32),
            pltpu.VMEM((4, rows, width), F32),
            pltpu.VMEM((4, rows, width), BF16),
            pltpu.VMEM((4, rows, width), BF16),
            pltpu.VMEM((6, rows, width // 2), BF16),
            pltpu.VMEM((6, rows, width // 2), BF16),
            pltpu.VMEM((rows, width), F32),
        ]
        + [slots] * 4
        + [
            pltpu.VMEM((chunk_rows, width), BF16),
            pltpu.VMEM((chunk_rows, gate.shape[1]), BF16),
            match,
            match,
            pltpu.SemaphoreType.DMA((9,)),
        ]
        + [pltpu.SemaphoreType.DMA((4,))] * 6
        + [pltpu.SemaphoreType.DMA((6,))] * 2
        + [pltpu.SemaphoreType.DMA((devices,))] * 4
    )
    return pl.pallas_call(
        layer_kernel,
        out_shape=jax.ShapeDtypeStruct((rows, width), BF16),
        in_specs=[pl.BlockSpec(memory_space=pltpu.VMEM)] * len(small)
        + [pl.BlockSpec(memory_space=pl.ANY)] * len(large),
        out_specs=pl.BlockSpec(memory_space=pltpu.VMEM),
        scratch_shapes=scratch,
        compiler_params=pltpu.CompilerParams(
            collective_id=0, has_side_effects=True, vmem_limit_bytes=60 * 1024 * 1024
        ),
        name="layer",
    )(*small, *large)


def local(
    residual,
    receptance_first,
    key_first_group,
    value_first_group,
    decay_preact_first,
    context_rate_first,
    decay_base_first,
    head_scale_first,
    receptance_second,
    key_second_group,
    value_second_group,
    decay_preact_second,
    context_rate_second,
    decay_base_second,
    head_scale_second,
    decay_extra_log,
    output_weight_first,
    output_weight_second,
    feedforward_gain,
    routed_expert_index,
    routed_expert_weight,
    expert_gate_weight,
    expert_up_weight,
    expert_down_weight,
    shared_gate_weight,
    shared_up_weight,
    shared_down_weight,
):
    small = (
        receptance_first,
        key_first_group,
        value_first_group,
        decay_preact_first,
        context_rate_first,
        decay_base_first[None, :],
        head_scale_first[None, :],
        receptance_second,
        key_second_group,
        value_second_group,
        decay_preact_second,
        context_rate_second,
        decay_base_second[None, :],
        head_scale_second[None, :],
        decay_extra_log.reshape(-1, SPAN),
        feedforward_gain[None, :],
        routed_expert_index.T,
        routed_expert_weight.T,
        slot_table(),
    )
    large = (
        residual,
        output_weight_first,
        output_weight_second,
        expert_gate_weight[0],
        expert_up_weight[0],
        expert_down_weight[0],
        shared_gate_weight,
        shared_up_weight,
        shared_down_weight,
    )
    return layer_call(small, large)


def solution(mesh):
    finer = Mesh(mesh.devices.reshape(4, 4, 4, 2), ALL)
    sp, tp = (Z, X), (Y, C)
    heads = (P(sp, tp),) * 5 + (P(tp),) * 2
    placed = (
        (P(ALL, None),)
        + heads
        + heads
        + (P(sp), P(tp, None), P(tp, None), P(), P(ALL, None), P(ALL, None))
        + (P(ALL, None, None),) * 3
        + (P(),) * 3
    )
    return jax.shard_map(
        local, mesh=finer, in_specs=placed, out_specs=P(ALL, None), check_vma=False
    )
```

time: 125 us -> 105 us (0.84); the launches traced: 123 us -> 105 us
  Pallas kernels: 119 us -> 103 us
  local copies, waits for them, and re-layouts: 3.55 us -> 1.67 us
    pallas_call x5 -> x1, Pallas kernels: 119 us -> 103 us  [layer_call(): pl.pallas_call(layer_kernel, out_shape=jax.ShapeDtypeStruct((rows, width)...]
    unnamed x19 -> x1, local copies, waits for them, and re-layouts: 3.55 us -> 1.67 us
where the time goes in v2:
time: 105 us
  Pallas kernels  103 us (98%)
  local copies, waits for them, and re-layouts  1.67 us (2%)
    pallas_call x1, Pallas kernels, layer_call(): pl.pallas_call(layer_kernel, out_shape=jax.ShapeDtypeStruct((rows, width)...  103 us

profile of v2, /device:TPU:1, one launch (start us, length us, event | category | flops | bytes accessed | tf_op | source)
XLA Modules:
  0.0 104.7 jit_solution(14113356698758537144)
XLA Ops:
  0.0 103.0 %layer.1 = bf16[64,2048]{1,0:T(8,128)(2,1)} custom-call(bf16[512,128]{1,0:T(8,128)(2,1)} %r_a.1, bf16[512,128]{1,0:T(8,128)(2,1)} %k_a.1, bf16[512,128]{1,0:T(8,128)(2,1)} %v_a.1, bf16[512,128]{1,0:T(8,128)(2,1)} %p_a.1, bf16[512,128]{1,0:T(8,128)(2,1)} %c_a.1, f32[1,128]{1,0:T(1,128)} %bitcast.18, f32[1,128]{1,0:T(1,128)} %bitcast.19, ...), custom_call_target="tpu_custom_call" | custom-call | tf_op jit(solution)/shard_map/layer/pallas_call | solution.py:677
  103.1 1.7 %copy.30 = bf16[64,2048]{1,0:T(8,128)(2,1)} copy(bf16[64,2048]{1,0:T(8,128)(2,1)} %layer.1) | data formatting | bytes 524288

commit v3 on v2

--- a/solution.py
+++ b/solution.py
@@ -25,16 +25,17 @@
 UNIT = SLOTS * PARTS
 GROUP = 256
 CHUNKS = 4
+WINDOW = 4
 
 
 def distance(move):
     return sum(min(step, 4 - step) for step in move[:3])
 
 
-MOVES = sorted(
-    itertools.product(range(4), range(4), range(4), range(2)),
-    key=lambda move: (-distance(move), -move[3]),
-)
+MOVES = sorted(itertools.product(range(4), range(4), range(4), range(2)), key=lambda move: (not any(move), (move[0]*32+move[1]*8+move[2]*2+move[3])*37%128))
+
+
+LINES = [move for move in MOVES if sum(step > 0 for step in move) == 1]
 
 
 def nn(a, b):
@@ -308,7 +309,7 @@
     z, x, y, c = position = tuple(lax.axis_index(name) for name in ALL)
     devices = len(MOVES)
     barrier = pltpu.get_barrier_semaphore()
-    for move in MOVES[:-1]:
+    for move in LINES:
         pl.semaphore_signal(
             barrier, inc=1, device_id=shift(position, move, 1), device_id_type=MESH
         )
@@ -347,7 +348,7 @@
     block_steps(items)
     chains = [[item for item in items if item["group"] == group] for group in range(2)]
     pack(message, *[block_chain(chain) for chain in chains])
-    pl.semaphore_wait(barrier, devices - 1)
+    pl.semaphore_wait(barrier, len(LINES))
 
     def row_copy(d):
         goal = (z, lax.rem(x + d, 4), y, c)
@@ -534,6 +535,11 @@
         found = (iota((GROUP, LANES), 0) + GROUP * k) // UNIT == iota((GROUP, LANES), 1)
         return jnp.where(found, 1.0, 0.0).astype(BF16)
 
+    span = groups // CHUNKS
+
+    def chunk_slots(k):
+        return range(per * span * k, min(per * span * (k + 1), devices - 1))
+
     def launch(k):
         for slot in range(per * k, min(per * (k + 1), devices - 1)):
             out_copy(slot).start()
@@ -542,9 +548,10 @@
         found = nt(select(k), code)
         taken = jnp.where(fits & (found == wanted), 1.0, 0.0).astype(BF16)
         sent[GROUP * k : GROUP * (k + 1), :] = nn(taken, stacked).astype(BF16)
-        if k:
+        if 0 < k <= WINDOW * span:
             launch(k - 1)
-    launch(groups - 1)
+    if WINDOW * span >= groups:
+        launch(groups - 1)
     arrived[unit(devices - 1), :] = sent[unit(devices - 1), :]
 
     for load in loads[3:5]:
@@ -573,11 +580,6 @@
     order_back = jnp.where(b == there, 1.0, 0.0).astype(BF16)
     for load in loads[6:]:
         load.wait()
-
-    span = groups // CHUNKS
-
-    def chunk_slots(k):
-        return range(per * span * k, min(per * span * (k + 1), devices - 1))
 
     for chunk in range(CHUNKS):
         for slot in chunk_slots(chunk):
@@ -604,6 +606,11 @@
             back[GROUP * k : GROUP * (k + 1), :] = nn(order_back, gathered).astype(BF16)
         for slot in chunk_slots(chunk):
             back_copy(slot).start()
+        if chunk + WINDOW < CHUNKS:
+            for slot in chunk_slots(chunk):
+                out_copy(slot).wait_send()
+            for slot in chunk_slots(chunk + WINDOW):
+                out_copy(slot).start()
     returned[unit(devices - 1), :] = back[unit(devices - 1), :]
 
     routed = jnp.zeros((PARTS * rows, part), F32)
@@ -621,9 +628,11 @@
         def _():
             col_copy(d).wait_send()
 
-    for slot in range(devices - 1):
-        out_copy(slot).wait_send()
-        back_copy(slot).wait_send()
+    for chunk in range(CHUNKS):
+        for slot in chunk_slots(chunk):
+            if chunk + WINDOW >= CHUNKS:
+                out_copy(slot).wait_send()
+            back_copy(slot).wait_send()
 
 
 def slot_table():

time: 105 us -> 92.9 us (0.88)
  Pallas kernels: 103 us -> 91 us
    pallas_call x1, Pallas kernels: 103 us -> 91 us  [layer_call(): pl.pallas_call(layer_kernel, out_shape=jax.ShapeDtypeStruct((rows, width)...]
where the time goes in v3:
time: 92.9 us; the launch traced here: 92.7 us
  Pallas kernels  91 us (98%)
  local copies, waits for them, and re-layouts  1.67 us (2%)
    pallas_call x1, Pallas kernels, layer_call(): pl.pallas_call(layer_kernel, out_shape=jax.ShapeDtypeStruct((rows, width)...  91 us

profile of v3, /device:TPU:1, one launch (start us, length us, event | category | flops | bytes accessed | tf_op | source)
XLA Modules:
  0.0 92.7 jit_solution(8274621872883146825)
XLA Ops:
  0.0 91.0 %layer.1 = bf16[64,2048]{1,0:T(8,128)(2,1)} custom-call(bf16[512,128]{1,0:T(8,128)(2,1)} %r_a.1, bf16[512,128]{1,0:T(8,128)(2,1)} %k_a.1, bf16[512,128]{1,0:T(8,128)(2,1)} %v_a.1, bf16[512,128]{1,0:T(8,128)(2,1)} %p_a.1, bf16[512,128]{1,0:T(8,128)(2,1)} %c_a.1, f32[1,128]{1,0:T(1,128)} %bitcast.18, f32[1,128]{1,0:T(1,128)} %bitcast.19, ...), custom_call_target="tpu_custom_call" | custom-call | tf_op jit(solution)/shard_map/layer/pallas_call | solution.py:686
  91.0 1.7 %copy.30 = bf16[64,2048]{1,0:T(8,128)(2,1)} copy(bf16[64,2048]{1,0:T(8,128)(2,1)} %layer.1) | data formatting | bytes 524288

commit v4 on v3

--- a/solution.py
+++ b/solution.py
@@ -24,15 +24,16 @@
 PARTS = 4
 UNIT = SLOTS * PARTS
 GROUP = 256
-CHUNKS = 4
-WINDOW = 4
+CHUNKS = 8
+WINDOW = 8
 
 
 def distance(move):
     return sum(min(step, 4 - step) for step in move[:3])
 
 
-MOVES = sorted(itertools.product(range(4), range(4), range(4), range(2)), key=lambda move: (not any(move), (move[0]*32+move[1]*8+move[2]*2+move[3])*37%128))
+MOVES = [[3, 3, 3, 1], [1, 0, 3, 1], [2, 2, 3, 0], [1, 1, 1, 0], [1, 2, 1, 1], [0, 0, 2, 1], [1, 1, 3, 0], [3, 3, 2, 0], [1, 1, 2, 0], [1, 0, 2, 1], [2, 3, 3, 1], [0, 1, 3, 1], [3, 3, 1, 0], [3, 2, 0, 1], [0, 2, 3, 0], [3, 0, 0, 0], [0, 1, 0, 0], [0, 2, 0, 1], [0, 3, 0, 1], [1, 1, 0, 0], [0, 2, 2, 1], [3, 2, 2, 0], [3, 1, 2, 0], [2, 2, 0, 1], [3, 0, 2, 0], [0, 2, 3, 1], [0, 1, 1, 0], [2, 3, 0, 0], [2, 2, 3, 1], [3, 0, 3, 0], [1, 2, 2, 0], [2, 2, 0, 0], [2, 3, 3, 0], [1, 1, 3, 1], [1, 0, 1, 0], [0, 1, 1, 1], [0, 0, 3, 1], [1, 3, 3, 0], [2, 1, 1, 1], [0, 0, 3, 0], [2, 1, 2, 1], [1, 0, 2, 0], [2, 0, 2, 1], [0, 1, 2, 0], [1, 3, 2, 0], [3, 2, 0, 0], [1, 2, 2, 1], [1, 2, 0, 0], [2, 0, 1, 1], [0, 3, 3, 1], [2, 1, 0, 0], [3, 1, 1, 0], [0, 3, 1, 0], [3, 1, 3, 0], [1, 0, 0, 0], [2, 2, 1, 1], [0, 2, 1, 1], [0, 2, 2, 0], [2, 3, 0, 1], [2, 0, 1, 0], [2, 1, 1, 0], [2, 1, 3, 1], [3, 3, 0, 1], [2, 2, 2, 1], [2, 0, 0, 1], [1, 1, 1, 1], [3, 3, 0, 0], [3, 3, 3, 0], [0, 3, 0, 0], [3, 1, 3, 1], [1, 2, 3, 0], [2, 3, 2, 0], [1, 0, 3, 0], [1, 3, 1, 1], [2, 2, 1, 0], [3, 1, 0, 1], [1, 1, 2, 1], [3, 0, 0, 1], [2, 0, 3, 1], [3, 2, 3, 1], [1, 3, 0, 1], [0, 3, 2, 1], [2, 0, 2, 0], [2, 3, 1, 1], [1, 2, 3, 1], [0, 3, 2, 0], [3, 2, 1, 0], [0, 0, 1, 0], [2, 0, 3, 0], [3, 2, 1, 1], [3, 1, 0, 0], [0, 0, 1, 1], [3, 3, 2, 1], [1, 1, 0, 1], [0, 1, 3, 0], [2, 1, 2, 0], [0, 3, 3, 0], [2, 3, 2, 1], [1, 0, 1, 1], [3, 2, 2, 1], [2, 3, 1, 0], [0, 0, 0, 1], [3, 0, 1, 1], [3, 2, 3, 0], [2, 1, 3, 0], [1, 3, 0, 0], [1, 2, 1, 0], [3, 1, 1, 1], [0, 0, 2, 0], [1, 3, 3, 1], [0, 1, 2, 1], [0, 3, 1, 1], [3, 0, 2, 1], [1, 2, 0, 1], [2, 2, 2, 0], [1, 3, 2, 1], [1, 3, 1, 0], [3, 3, 1, 1], [2, 0, 0, 0], [0, 2, 0, 0], [1, 0, 0, 1], [0, 1, 0, 1], [3, 0, 1, 0], [3, 0, 3, 1], [3, 1, 2, 1], [2, 1, 0, 1], [0, 2, 1, 0], [0, 0, 0, 0]]
+MOVES = [tuple(move) for move in MOVES]
 
 
 LINES = [move for move in MOVES if sum(step > 0 for step in move) == 1]

time: 92.9 us -> 92.9 us (level)
  no operation moved by 1% of the time
where the time goes in v4:
time: 92.9 us; the launch traced here: 92.6 us
  Pallas kernels  90.9 us (98%)
  local copies, waits for them, and re-layouts  1.67 us (2%)
    pallas_call x1, Pallas kernels, layer_call(): pl.pallas_call(layer_kernel, out_shape=jax.ShapeDtypeStruct((rows, width)...  90.9 us

profile of v4, /device:TPU:1, one launch (start us, length us, event | category | flops | bytes accessed | tf_op | source)
XLA Modules:
  0.0 92.6 jit_solution(9513193617975671779)
XLA Ops:
  0.0 90.9 %layer.1 = bf16[64,2048]{1,0:T(8,128)(2,1)} custom-call(bf16[512,128]{1,0:T(8,128)(2,1)} %r_a.1, bf16[512,128]{1,0:T(8,128)(2,1)} %k_a.1, bf16[512,128]{1,0:T(8,128)(2,1)} %v_a.1, bf16[512,128]{1,0:T(8,128)(2,1)} %p_a.1, bf16[512,128]{1,0:T(8,128)(2,1)} %c_a.1, f32[1,128]{1,0:T(1,128)} %bitcast.18, f32[1,128]{1,0:T(1,128)} %bitcast.19, ...), custom_call_target="tpu_custom_call" | custom-call | tf_op jit(solution)/shard_map/layer/pallas_call | solution.py:687
  90.9 1.7 %copy.30 = bf16[64,2048]{1,0:T(8,128)(2,1)} copy(bf16[64,2048]{1,0:T(8,128)(2,1)} %layer.1) | data formatting | bytes 524288
